TPU v7x, 256 devices: a 4x2x16 block of a 4x16x16 slice. The times are simulated.
256 devices in a mesh: grp: 2 (over y), ep: 64 (over z, x), tp: 2 (over core).
Axes of the slice: x: 4, y: 2, z: 16, core: 2. Of those that a mesh axis runs over, the one named last changes fastest.
The devices are a block of a 4x16x16 slice.
Arguments:
- hidden: bfloat16 [1024, 2048], P(('grp', 'ep'), 'tp'), parts along dimension 0, may hold values from -6 to 6
- head_input_projected: bfloat16 [1024, 2048], P(('grp', 'ep'), 'tp'), parts along dimension 0, may hold values from -6 to 6
- output_gate_projected: bfloat16 [1024, 2048], P(('grp', 'ep'), 'tp'), parts along dimension 0, may hold values from -6 to 6
- input_map_projected: bfloat16 [1024, 256], P(('grp', 'ep'), 'tp'), parts along dimension 0, may hold values from -0.59765625 to 0.59765625
- output_map_projected: bfloat16 [1024, 256], P(('grp', 'ep'), 'tp'), parts along dimension 0, may hold values from -6 to 6
- raw_step_size: bfloat16 [1024, 32], P(('grp', 'ep'), 'tp'), parts along dimension 0, may hold values from -5 to 5
- convolution_history: bfloat16 [1024, 3, 2048], P(('grp', 'ep'), None, 'tp'), parts along dimension 0, may hold values from -6 to 6
- convolution_kernel: bfloat16 [4, 2048], P(None, 'tp'), may hold values from -3 to 3
- recurrent_state_matrix: float32 [1024, 32, 64, 64], P(('grp', 'ep'), 'tp'), parts along dimension 0, may hold values from -0.6 to 0.6
- head_decay_rate: float32 [32], P('tp'), may hold values from 0.05 to 4
- extra_log_decay: float32 [1024, 32], P(('grp', 'ep'), 'tp'), parts along dimension 0, may hold values from -0.7 to 0
- head_skip_weight: float32 [32], P('tp'), may hold values from 0.1 to 1.9
- output_matrix: bfloat16 [2048, 2048], P('tp'), may hold values from -0.125 to 0.125
- expert_norm_scale: bfloat16 [2048], replicated, may hold values from 0.099609375 to 1.8984375
- token_expert_index: int32 [1024, 6], P(('grp', 'ep')), parts along dimension 0, may hold values from 0 to 63, all different within a row; in each aligned block of 8 rows (0 to 7, 8 to 15, ...) at most 2 rows name the same one
- token_expert_weight: float32 [1024, 6], P(('grp', 'ep')), parts along dimension 0, may hold values from 0.2 to 1
- expert_gate_weight: bfloat16 [64, 2048, 704], P('ep', None, 'tp'), may hold values from -0.125 to 0.125
- expert_up_weight: bfloat16 [64, 2048, 704], P('ep', None, 'tp'), may hold values from -0.125 to 0.125
- expert_down_weight: bfloat16 [64, 704, 2048], P('ep', 'tp'), may hold values from -0.21875 to 0.21875
Outputs:
- layer_out: bfloat16 [1024, 2048], P(('grp', 'ep'), 'tp'), parts along dimension 0
- new_state: float32 [1024, 32, 64, 64], P(('grp', 'ep'), 'tp'), parts along dimension 0
- new_hist: bfloat16 [1024, 3, 2048], P(('grp', 'ep'), None, 'tp'), parts along dimension 0
There are 2 independent parts, one for each index of `grp`. A program takes and returns all parts, laid end to end along the dimension named above; an argument that names none is the same for every part. Nothing has to cross between parts.
Inputs may be any that keep to these rules, and one draw needn't show every extreme that they name: `token_expert_index`: in the rows of one device (8 rows), no expert is named more than 2 times, and one expert is named exactly 2 times in some blocks; a token names 6 different experts.
All inputs are finite; a program needn't handle non-finite values.
Results may differ from a plain program's by a relative error of at most 0.015.
Values may be sent and summed in bfloat16 or wider, within the bound.
A program may use at most 64 MiB of HBM per device.

v0:
```python
import jax
import jax.numpy as jnp
from jax import lax
from jax.sharding import PartitionSpec as P

STATE_DIM = 64
TOPK = 6


EPSILON = 1e-06


def in_blocks(value, dim, length):
    dims = value.shape
    pieces = value.reshape(*dims[:dim], length, dims[dim] // length, *dims[dim + 1 :])
    return jnp.moveaxis(pieces, dim, 0)


def sent_and_summed(value, axis, dim):
    pieces = in_blocks(value, dim, lax.axis_size(axis))
    arrived = lax.all_to_all(pieces, axis, split_axis=0, concat_axis=0, tiled=True)
    return arrived.astype(jnp.float32).sum(axis=0)


def slot_numbers(token_expert_index, capacity, experts):
    flat = token_expert_index.reshape(-1)
    onehot = (flat[:, None] == jnp.arange(experts, dtype=jnp.int32)[None, :]).astype(jnp.int32)
    before = jnp.cumsum(onehot, axis=0) - onehot
    ranks = jnp.sum(before * onehot, axis=1)
    return (flat * capacity + ranks).reshape(token_expert_index.shape)


def on_device(
    hidden,
    head_input_projected,
    output_gate_projected,
    input_map_projected,
    output_map_projected,
    raw_step_size,
    convolution_history,
    convolution_kernel,
    recurrent_state_matrix,
    head_decay_rate,
    extra_log_decay,
    head_skip_weight,
    output_matrix,
    expert_norm_scale,
    token_expert_index,
    token_expert_weight,
    expert_gate_weight,
    expert_up_weight,
    expert_down_weight,
):
    seq_count, inner_local = head_input_projected.shape
    heads_local = raw_step_size.shape[1]
    head_width = inner_local // heads_local
    groups_local = input_map_projected.shape[1] // STATE_DIM
    per_group = heads_local // groups_local
    half_width = hidden.shape[1]
    ep_count = lax.axis_size("ep")
    window = jnp.concatenate([convolution_history, head_input_projected[:, None, :]], axis=1)
    new_hist = window[:, 1:]
    conv = jax.nn.silu(
        jnp.sum(window.astype(jnp.float32) * convolution_kernel.astype(jnp.float32)[None], axis=1)
    )
    positive_step_size = jax.nn.softplus(raw_step_size.astype(jnp.float32))
    decay_factor = jnp.exp(-head_decay_rate[None, :] * positive_step_size + extra_log_decay)
    heads_in = conv.reshape(seq_count, heads_local, head_width)
    b_heads = jnp.repeat(
        input_map_projected.astype(jnp.float32).reshape(seq_count, groups_local, STATE_DIM),
        per_group,
        axis=1,
    )
    c_heads = jnp.repeat(
        output_map_projected.astype(jnp.float32).reshape(seq_count, groups_local, STATE_DIM),
        per_group,
        axis=1,
    )
    new_state = (
        decay_factor[:, :, None, None] * recurrent_state_matrix
        + (positive_step_size[:, :, None] * heads_in)[:, :, :, None] * b_heads[:, :, None, :]
    )
    readout = (
        jnp.einsum("shpn,shn->shp", new_state, c_heads) + head_skip_weight[None, :, None] * heads_in
    )
    gated = (
        readout.reshape(seq_count, inner_local)
        * jax.nn.silu(output_gate_projected.astype(jnp.float32))
    ).astype(jnp.bfloat16)
    partial_value = jnp.dot(gated, output_matrix, preferred_element_type=jnp.float32)
    mixed = sent_and_summed(partial_value.astype(jnp.bfloat16), "tp", 1)
    resid = (hidden.astype(jnp.float32) + mixed).astype(jnp.bfloat16)
    capacity = min(seq_count, max(2, 2 * seq_count * TOPK // ep_count))
    total_slots = ep_count * capacity
    slot_ids = jnp.arange(total_slots, dtype=jnp.int32)
    slots = slot_numbers(token_expert_index, capacity, ep_count)
    hits = (slots[:, :, None] == slot_ids[None, None, :]).astype(jnp.float32)
    picks = jnp.sum(hits, axis=1).T.astype(jnp.bfloat16)
    outgoing = jnp.dot(picks, resid, preferred_element_type=jnp.float32).astype(jnp.bfloat16)
    received = lax.all_to_all(
        outgoing.reshape(ep_count, capacity, half_width),
        "ep",
        split_axis=0,
        concat_axis=0,
        tiled=True,
    )
    expert_rows = lax.all_gather(
        received.reshape(total_slots, half_width), "tp", axis=1, tiled=True
    )
    values = expert_rows.astype(jnp.float32)
    inv_rms = lax.rsqrt(jnp.mean(values * values, axis=1, keepdims=True) + EPSILON)
    scaled = (values * expert_norm_scale.astype(jnp.float32)[None, :]).astype(jnp.bfloat16)
    pre_gate = inv_rms * jnp.dot(scaled, expert_gate_weight[0], preferred_element_type=jnp.float32)
    pre_up = inv_rms * jnp.dot(scaled, expert_up_weight[0], preferred_element_type=jnp.float32)
    act = (jax.nn.silu(pre_gate) * pre_up).astype(jnp.bfloat16)
    down_part = jnp.dot(act, expert_down_weight[0], preferred_element_type=jnp.float32)
    expert_out = sent_and_summed(down_part.astype(jnp.bfloat16), "tp", 1).astype(jnp.bfloat16)
    back = lax.all_to_all(
        expert_out.reshape(ep_count, capacity, half_width),
        "ep",
        split_axis=0,
        concat_axis=0,
        tiled=True,
    )
    mixing = jnp.sum(hits * token_expert_weight[:, :, None], axis=1)
    routed = jnp.dot(mixing, back.reshape(total_slots, half_width).astype(jnp.float32))
    layer_out = (resid.astype(jnp.float32) + routed).astype(jnp.bfloat16)
    return (layer_out, new_state, new_hist)


def solution(mesh):
    in_specs = (
        P(("grp", "ep"), "tp"),
        P(("grp", "ep"), "tp"),
        P(("grp", "ep"), "tp"),
        P(("grp", "ep"), "tp"),
        P(("grp", "ep"), "tp"),
        P(("grp", "ep"), "tp"),
        P(("grp", "ep"), None, "tp"),
        P(None, "tp"),
        P(("grp", "ep"), "tp", None, None),
        P("tp"),
        P(("grp", "ep"), "tp"),
        P("tp"),
        P("tp", None),
        P(),
        P(("grp", "ep"), None),
        P(("grp", "ep"), None),
        P("ep", None, "tp"),
        P("ep", None, "tp"),
        P("ep", "tp", None),
    )
    out_specs = (
        P(("grp", "ep"), "tp"),
        P(("grp", "ep"), "tp", None, None),
        P(("grp", "ep"), None, "tp"),
    )
    return jax.shard_map(
        on_device, mesh=mesh, in_specs=in_specs, out_specs=out_specs, check_vma=False
    )
```

profile of v0, /device:TPU:40, one launch (start us, length us, event | category | flops | bytes accessed | tf_op | source)
XLA Modules:
  0.0 114.0 jit_solution(18267594604967208549)
XLA Ops:
  0.6 0.9 reshape.95
  1.5 0.7 neg.24
  2.2 0.7 convert_element_type.69
  2.9 0.8 multiply_reduce_fusion
  3.8 0.8 reshape.97
  4.6 0.7 add_exponential_fusion
  5.4 3.8 %multiply_add_fusion = f32[8,16,64,64]{3,2,1,0:T(8,128)S(1)} fusion(f32[8,16,64,64]{3,2,1,0:T(8,128)} %param.27, f32[8,16,64]{2,1,0:T(8,128)S(1)} %broadcast_bitcast_fusion, f32[8,16,64]{2,1,0:T(8,128)S(1)} %broadcast_multiply_fusion, f32[8,16]{1,0:T(8,128)S(1)} %get-tuple-element.5), kind=kLoop, calls=%fused_computation | loop fusion | flops 1572864 | bytes 4260352 | tf_op jit(solution)/shard_map/add | solution.py:80
  9.2 2.0 %copy-done.1 = f32[8,16,64,64]{3,2,1,0:T(8,128)} copy-done((f32[8,16,64,64]{3,2,1,0:T(8,128)}, f32[8,16,64,64]{3,2,1,0:T(8,128)S(1)}, u32[]{:S(2)}) %copy-start.1) | copy-done | bytes 2097176
  11.2 1.2 %fusion.48 = f32[8,16,1,64]{3,2,1,0:T(1,128)S(1)} fusion(f32[8,16,64,64]{3,2,1,0:T(8,128)S(1)} %multiply_add_fusion, f32[8,16,64,1]{2,3,1,0:T(1,128)S(1)} %bitcast.48), kind=kOutput, calls=%fused_computation.65 | convolution fusion | flops 1048576 | bytes 2162688 | tf_op jit(solution)/shard_map/shpn,shn->shp/dot_general | solution.py:84
  12.5 3.5 %convolution_convert_fusion.1 = bf16[8,2048]{1,0:T(8,128)(2,1)} fusion(bf16[1024,2048]{1,0:T(8,128)(2,1)} %param.31, f32[8,1024]{1,0:T(8,128)S(1)} %reshape.87, bf16[8,1024]{1,0:T(8,128)(2,1)S(1)} %copy-done.6), kind=kOutput, calls=%fused_computation.2 | convolution fusion | flops 33628160 | bytes 4276224 | tf_op jit(solution)/shard_map/dot_general | solution.py:90
  16.1 3.3 %all-to-all-start = ((bf16[2,8,1024]{2,1,0:T(8,128)(2,1)}), bf16[2,8,1024]{2,1,0:T(8,128)(2,1)S(1)}, u32[]{:S(2)}, u32[]{:S(2)}) async-start(bf16[2,8,1024]{2,1,0:T(8,128)(2,1)} %bitcast.8), calls=%async_computation | async-start | bytes 65536 | tf_op jit(solution)/shard_map/all_to_all | solution.py:21
  21.0 0.8 reshape.89
  21.8 29.0 %all-to-all-start.1 = ((bf16[64,2,1024]{2,1,0:T(2,128)(2,1)}), bf16[64,2,1024]{2,1,0:T(2,128)(2,1)S(1)}, u32[]{:S(2)}, u32[]{:S(2)}) async-start(bf16[64,2,1024]{2,1,0:T(2,128)(2,1)} %reshape.89), calls=%async_computation.1 | async-start | bytes 524288 | tf_op jit(solution)/shard_map/all_to_all | solution.py:100
  50.9 21.5 %all-to-all-done.1 = bf16[64,2,1024]{2,1,0:T(2,128)(2,1)S(1)} async-done(((bf16[64,2,1024]{2,1,0:T(2,128)(2,1)}), bf16[64,2,1024]{2,1,0:T(2,128)(2,1)S(1)}, u32[]{:S(2)}, u32[]{:S(2)}) %all-to-all-start.1) | async-done | bytes 262176 | tf_op jit(solution)/shard_map/all_to_all | solution.py:100
  72.3 0.8 reshape.90
  73.1 2.4 %all_gather.3 = bf16[128,2048]{1,0:T(8,128)(2,1)S(1)} all-gather(bf16[128,1024]{1,0:T(8,128)(2,1)} %reshape.90), channel_id=1, replica_groups=mesh['grp'=2,'ep'=64,'tp'=2] {'tp'}, dimensions={1}, use_global_device_ids=true | all-gather | bytes 786432 | tf_op jit(solution)/shard_map/all_gather | solution.py:107
  75.7 1.2 %fusion.5 = f32[128,352]{0,1:T(8,128)} fusion(bf16[1,2048,352]{1,2,0:T(8,128)(2,1)S(1)} %copy-done.2, bf16[128,2048]{1,0:T(8,128)(2,1)S(1)} %all_gather.3, f32[2048]{0:T(1024)S(1)} %convert_element_type.81, f32[128]{0:T(128)S(1)} %add_rsqrt_fusion), kind=kOutput, calls=%fused_computation.11 | convolution fusion | flops 185380864 | bytes 2155008 | tf_op jit(solution)/shard_map/dot_general | solution.py:113
  77.0 2.8 %convolution_convert_fusion = bf16[128,2048]{1,0:T(8,128)(2,1)S(1)} fusion(bf16[1,352,2048]{2,1,0:T(8,128)(2,1)S(1)} %copy-done, bf16[1,2048,352]{1,2,0:T(8,128)(2,1)} %param.36, bf16[128,2048]{1,0:T(8,128)(2,1)S(1)} %all_gather.3, f32[2048]{0:T(1024)S(1)} %convert_element_type.81, f32[128,352]{0,1:T(8,128)} %fusion.5, f32[128]{0:T(128)S(1)} %add_rsqrt_fusion), kind=kOutput, calls=%fused_computation.1 | convolution fusion | flops 370462720 | bytes 4121088 | tf_op jit(solution)/shard_map/dot_general | solution.py:116
  79.9 4.2 %all_to_all.20 = bf16[2,128,1024]{2,1,0:T(8,128)(2,1)S(1)} all-to-all(bf16[2,128,1024]{2,1,0:T(8,128)(2,1)S(1)} %bitcast.46), channel_id=1, replica_groups=mesh['grp'=2,'ep'=64,'tp'=2] {'tp'}, dimensions={0} | all-to-all | bytes 1048576 | tf_op jit(solution)/shard_map/all_to_all | solution.py:21
  84.1 0.8 reshape.92
  84.9 6.5 %all-to-all-start.3 = ((bf16[64,2,1024]{2,1,0:T(2,128)(2,1)}), bf16[64,2,1024]{2,1,0:T(2,128)(2,1)S(1)}, u32[]{:S(2)}, u32[]{:S(2)}) async-start(bf16[64,2,1024]{2,1,0:T(2,128)(2,1)} %reshape.92), calls=%async_computation.3 | async-start | bytes 524288 | tf_op jit(solution)/shard_map/all_to_all | solution.py:118
  91.4 0.6 fusion.32
  92.1 21.1 %all-to-all-done.3 = bf16[64,2,1024]{2,1,0:T(2,128)(2,1)S(1)} async-done(((bf16[64,2,1024]{2,1,0:T(2,128)(2,1)}), bf16[64,2,1024]{2,1,0:T(2,128)(2,1)S(1)}, u32[]{:S(2)}, u32[]{:S(2)}) %all-to-all-start.3) | async-done | bytes 262176 | tf_op jit(solution)/shard_map/all_to_all | solution.py:118
  113.3 0.8 fusion.19
  (45 shorter events, 2.5 us)
Async XLA Ops:
  0.6 76.3 %copy-start = (bf16[1,352,2048]{2,1,0:T(8,128)(2,1)S(1)}, bf16[1,352,2048]{2,1,0:T(8,128)(2,1)}, u32[]{:S(2)}) copy-start(bf16[1,352,2048]{2,1,0:T(8,128)(2,1)} %param.37) | copy-start | bytes 4325380
  9.1 2.0 %copy-start.1 = (f32[8,16,64,64]{3,2,1,0:T(8,128)}, f32[8,16,64,64]{3,2,1,0:T(8,128)S(1)}, u32[]{:S(2)}) copy-start(f32[8,16,64,64]{3,2,1,0:T(8,128)S(1)} %multiply_add_fusion) | copy-start | bytes 6291460
  9.2 3.2 %copy-start.10 = (f32[16]{0:T(128)S(1)}, f32[16]{0:T(128)}, u32[]{:S(2)}) copy-start(f32[16]{0:T(128)} %param.30) | copy-start | bytes 196
  9.2 3.4 %copy-start.6 = (bf16[8,1024]{1,0:T(8,128)(2,1)S(1)}, bf16[8,1024]{1,0:T(8,128)(2,1)}, u32[]{:S(2)}) copy-start(bf16[8,1024]{1,0:T(8,128)(2,1)} %param.21) | copy-start | bytes 49156
  11.2 8.2 %copy-start.7 = (s32[8,6]{1,0:T(8,128)S(1)}, s32[8,6]{1,0:T(8,128)}, u32[]{:S(2)}) copy-start(s32[8,6]{1,0:T(8,128)} %param.33) | copy-start | bytes 580
  11.2 8.8 %copy-start.9 = (f32[8,6]{1,0:T(8,128)S(1)}, f32[8,6]{1,0:T(8,128)}, u32[]{:S(2)}) copy-start(f32[8,6]{1,0:T(8,128)} %param.34) | copy-start | bytes 580
  11.2 9.6 %copy-start.5 = (bf16[8,1024]{1,0:T(8,128)(2,1)S(1)}, bf16[8,1024]{1,0:T(8,128)(2,1)}, u32[]{:S(2)}) copy-start(bf16[8,1024]{1,0:T(8,128)(2,1)} %param.19) | copy-start | bytes 49156
  11.2 39.7 %copy-start.8 = (bf16[2048]{0:T(1024)(128)(2,1)S(1)}, bf16[2048]{0:T(1024)(128)(2,1)}, u32[]{:S(2)}) copy-start(bf16[2048]{0:T(1024)(128)(2,1)} %param.32) | copy-start | bytes 12292
  12.3 63.4 %copy-start.2 = (bf16[1,2048,352]{1,2,0:T(8,128)(2,1)S(1)}, bf16[1,2048,352]{1,2,0:T(8,128)(2,1)}, u32[]{:S(2)}) copy-start(bf16[1,2048,352]{1,2,0:T(8,128)(2,1)} %param.35) | copy-start | bytes 4325380
  16.1 4.7 %all-to-all-start = ((bf16[2,8,1024]{2,1,0:T(8,128)(2,1)}), bf16[2,8,1024]{2,1,0:T(8,128)(2,1)S(1)}, u32[]{:S(2)}, u32[]{:S(2)}) async-start(bf16[2,8,1024]{2,1,0:T(8,128)(2,1)} %bitcast.8), calls=%async_computation | async-start | bytes 65536 | tf_op jit(solution)/shard_map/all_to_all | solution.py:21
  21.8 50.5 %all-to-all-start.1 = ((bf16[64,2,1024]{2,1,0:T(2,128)(2,1)}), bf16[64,2,1024]{2,1,0:T(2,128)(2,1)S(1)}, u32[]{:S(2)}, u32[]{:S(2)}) async-start(bf16[64,2,1024]{2,1,0:T(2,128)(2,1)} %reshape.89), calls=%async_computation.1 | async-start | bytes 524288 | tf_op jit(solution)/shard_map/all_to_all | solution.py:100
  77.0 14.5 %copy-start.3 = (bf16[8,3,1024]{2,0,1:T(8,128)(2,1)S(1)}, bf16[8,3,1024]{2,0,1:T(8,128)(2,1)}, u32[]{:S(2)}) copy-start(bf16[8,3,1024]{2,0,1:T(8,128)(2,1)} %param.25) | copy-start | bytes 147460
  77.0 14.5 %copy-start.4 = (bf16[8,1024]{1,0:T(8,128)(2,1)S(1)}, bf16[8,1024]{1,0:T(8,128)(2,1)}, u32[]{:S(2)}) copy-start(bf16[8,1024]{1,0:T(8,128)(2,1)} %param.20) | copy-start | bytes 49156
  84.9 28.2 %all-to-all-start.3 = ((bf16[64,2,1024]{2,1,0:T(2,128)(2,1)}), bf16[64,2,1024]{2,1,0:T(2,128)(2,1)S(1)}, u32[]{:S(2)}, u32[]{:S(2)}) async-start(bf16[64,2,1024]{2,1,0:T(2,128)(2,1)} %reshape.92), calls=%async_computation.3 | async-start | bytes 524288 | tf_op jit(solution)/shard_map/all_to_all | solution.py:118
where the time goes:
time: 115 us; the launch traced here: 114 us
  waiting for transfers between devices  43.1 us (37%)
  starting transfers between devices  38.8 us (34%)
  matrix products  9.8 us (9%)
  other arithmetic  8.23 us (7%)
  local copies, waits for them, and re-layouts  6.65 us (6%)
  blocking collectives  6.58 us (6%)
    all_to_all x1, starting transfers between devices, on_device(): lax.all_to_all(outgoing.reshape(ep_count, capacity, half_width), 'ep', sp...  29 us
    all_to_all x1, waiting for transfers between devices, on_device(): lax.all_to_all(outgoing.reshape(ep_count, capacity, half_width), 'ep', sp...  21.5 us
    all_to_all x1, waiting for transfers between devices, on_device(): lax.all_to_all(expert_out.reshape(ep_count, capacity, half_width), 'ep',...  21.1 us
    all_to_all x1, starting transfers between devices, on_device(): lax.all_to_all(expert_out.reshape(ep_count, capacity, half_width), 'ep',...  6.48 us
    all_to_all x1, blocking collectives, sent_and_summed(): lax.all_to_all(pieces, axis, split_axis=0, concat_axis=0, tiled=True)  4.17 us
    add x1, other arithmetic, on_device(): decay_factor[:, :, None, None] * recurrent_state_matrix  3.76 us
    dot_general x1, matrix products, on_device(): jnp.dot(gated, output_matrix, preferred_element_type=jnp.float32)  3.55 us
    all_to_all x1, starting transfers between devices, sent_and_summed(): lax.all_to_all(pieces, axis, split_axis=0, concat_axis=0, tiled=True)  3.29 us
  transfers between devices with their start and end apart: 3, of which 3 were waited for; matrix products, arithmetic and copies ran while one was open for 1% of the time, Pallas kernels for 0%

commit v1 on v0

v1 whole, which is shorter than its diff:
```python
import functools

import jax
import jax.numpy as jnp
from jax import lax
from jax.experimental import pallas as pl
from jax.experimental.pallas import tpu as pltpu
from jax.sharding import PartitionSpec as P

MESH = pl.DeviceIdType.MESH
F32 = jnp.float32
BF16 = jnp.bfloat16

STATE_DIM = 64
TOPK = 6
CAP = 2
EPSILON = 1e-06
X_SIDE = 4
REACH = 4
LANES = 128
HIGH = lax.Precision.HIGHEST


def iota(shape, dim):
    return lax.broadcasted_iota(jnp.int32, shape, dim)


def silu(v):
    return v / (1.0 + jnp.exp(-v))


def softplus(v):
    return jnp.maximum(v, 0.0) + jnp.log1p(jnp.exp(-jnp.abs(v)))


def mixer_kernel(
    head_in, gate, b_map, c_map, raw_step, hist, taps, state, rate, extra, skip,
    new_state, new_hist, gated,
    conv_s, decay_s, u_t, y_s,
):
    step_at = pl.program_id(0)
    seqs, inner = head_in.shape
    heads = raw_step.shape[1]
    width = inner // heads
    groups = b_map.shape[1] // STATE_DIM
    per_group = heads // groups
    lanes_of = (iota((heads, inner), 1) // width == iota((heads, inner), 0)).astype(F32)

    @pl.when(step_at == 0)
    def _():
        x = head_in[...]
        for i in range(2):
            new_hist[i] = hist[i + 1]
        new_hist[2] = x
        kern = taps[...].astype(F32)
        total = x.astype(F32) * kern[3:4]
        for i in range(3):
            total = total + hist[i].astype(F32) * kern[i : i + 1]
        conv = silu(total)
        conv_s[...] = conv
        dt = softplus(raw_step[...].astype(F32))
        col = iota((seqs, heads), 1)
        rates = jnp.zeros((seqs, heads), F32)
        for h in range(heads):
            rates = jnp.where(col == h, rate[h], rates)
        decay_s[...] = jnp.exp(-rates * dt + extra[...])
        u = conv * jnp.dot(dt, lanes_of, precision=HIGH, preferred_element_type=F32)
        u_hi = u.astype(BF16).astype(F32)
        u_t[...] = jnp.concatenate([u_hi, u - u_hi], axis=0).T.astype(BF16)
        y_s[...] = jnp.zeros_like(y_s)

    row = iota((2 * seqs, STATE_DIM), 0)
    row_c = iota((seqs, STATE_DIM), 0)
    b_all = b_map[...]
    c_all = c_map[...]
    for g in range(groups):
        cols = slice(g * STATE_DIM, (g + 1) * STATE_DIM)
        b_g = jnp.concatenate([b_all[:, cols].astype(F32)] * 2, axis=0)
        b_g = jnp.where(row % seqs == step_at, b_g, 0.0).astype(BF16)
        c_g = jnp.where(row_c == step_at, c_all[:, cols].astype(F32), 0.0).astype(BF16)
        chans = per_group * width
        outer = jnp.dot(u_t[g * chans : (g + 1) * chans, :], b_g, preferred_element_type=F32)
        for j in range(per_group):
            h = g * per_group + j
            d = decay_s[pl.ds(step_at, 1), h : h + 1]
            new = d * state[0, h] + outer[j * width : (j + 1) * width]
            new_state[0, h] = new
        fresh = new_state[0, g * per_group : (g + 1) * per_group].reshape(chans, STATE_DIM)
        y_s[:, g * chans : (g + 1) * chans] += lax.dot_general(
            c_g, fresh.astype(BF16), (((1,), (1,)), ((), ())), preferred_element_type=F32
        )

    @pl.when(step_at == pl.num_programs(0) - 1)
    def _():
        col = iota((seqs, inner), 1) // width
        skips = jnp.zeros((seqs, inner), F32)
        for h in range(heads):
            skips = jnp.where(col == h, skip[h], skips)
        readout = y_s[...] + skips * conv_s[...]
        gated[...] = (readout * silu(gate[...].astype(F32))).astype(BF16)


def mixer(head_in, gate, b_map, c_map, raw_step, hist, taps, state, rate, extra, skip):
    seqs, inner = head_in.shape
    heads, width = state.shape[1:3]

    def whole(a):
        return pl.BlockSpec(a.shape, lambda i: (0,) * a.ndim)

    smem = pl.BlockSpec(memory_space=pltpu.SMEM)
    one = pl.BlockSpec((1,) + state.shape[1:], lambda i: (i, 0, 0, 0))
    return pl.pallas_call(
        mixer_kernel,
        name="mixer",
        grid=(seqs,),
        in_specs=[whole(head_in), whole(gate), whole(b_map), whole(c_map), whole(raw_step), whole(hist), whole(taps),
                  one, smem, whole(extra), smem],
        out_specs=[one, whole(hist), whole(head_in)],
        out_shape=[
            jax.ShapeDtypeStruct(state.shape, F32),
            jax.ShapeDtypeStruct(hist.shape, BF16),
            jax.ShapeDtypeStruct(head_in.shape, BF16),
        ],
        scratch_shapes=[
            pltpu.VMEM((seqs, inner), F32),
            pltpu.VMEM((seqs, heads), F32),
            pltpu.VMEM((inner, 2 * seqs), BF16),
            pltpu.VMEM((seqs, inner), F32),
        ],
        compiler_params=pltpu.CompilerParams(dimension_semantics=("arbitrary",)),
    )(head_in, gate, b_map, c_map, raw_step, hist, taps, state, rate, extra, skip)


def expert_kernel(
    gated, hidden, wout_h, norm, chosen, weights, wg_h, wu_h, wd_h,
    out,
    wout, wg, wu, wd, tp_tx, tp_rx, tokens, pick_tx, pick_rx, pick_other, down_tx, down_rx, back_tx, back_rx,
    sums, sums_bf, relay_rx, relay_tx, last_rx,
    w_sem, tp_s, tp_r, z_s, z_r, x_s, x_r, o_s, o_r, d_s, d_r, b_s, b_r, h_s, h_r,
):
    seqs, half = hidden.shape
    nz = tokens.shape[0]
    slots = nz * CAP
    rows = X_SIDE * slots
    me, core = lax.axis_index("ep"), lax.axis_index("tp")
    z, x = me // X_SIDE, me % X_SIDE
    other = 1 - core

    def along_z(d):
        return {"ep": ((z + d + nz) % nz) * X_SIDE + x}

    def along_x(d):
        return {"ep": z * X_SIDE + (x + d) % X_SIDE}

    partner = {"tp": other}
    mine_cols = pl.ds(pl.multiple_of(core * half, half), half)
    other_cols = pl.ds(pl.multiple_of(other * half, half), half)

    loads = [
        pltpu.make_async_copy(wout_h, wout, w_sem.at[0]),
        pltpu.make_async_copy(wg_h.at[0], wg, w_sem.at[1]),
        pltpu.make_async_copy(wu_h.at[0], wu, w_sem.at[2]),
        pltpu.make_async_copy(wd_h.at[0], wd, w_sem.at[3]),
    ]
    for load in loads:
        load.start()

    barrier = pltpu.get_barrier_semaphore()
    z_steps = [s * d for d in range(REACH, 0, -1) for s in (1, -1)]
    peers = [along_z(d) for d in z_steps] + [along_x(d) for d in range(1, X_SIDE)] + [partner]
    for peer in peers:
        pl.semaphore_signal(barrier, inc=1, device_id=peer, device_id_type=MESH)

    idx = chosen[...]
    wts = weights[...]
    lane = iota((seqs, LANES), 1)
    named = jnp.zeros((seqs, LANES), F32)
    for i in range(TOPK):
        named = named + (lane == idx[:, i : i + 1]).astype(F32)
    before = (iota((seqs, seqs), 1) < iota((seqs, seqs), 0)).astype(BF16)
    rank = jnp.dot(before, named.astype(BF16), preferred_element_type=F32)
    extra = jnp.zeros((seqs, LANES), F32)
    for i in range(TOPK):
        expert = idx[:, i : i + 1]
        place = jnp.sum(jnp.where(lane == expert, rank, 0.0), axis=1, keepdims=True)
        slot = expert.astype(F32) * CAP + place
        w = wts[:, i : i + 1]
        w_hi = w.astype(BF16).astype(F32)
        extra = jnp.where(lane == i, slot, extra)
        extra = jnp.where(lane == TOPK + i, w_hi, extra)
        extra = jnp.where(lane == 2 * TOPK + i, w - w_hi, extra)
    tokens[z, :, half:] = extra.astype(BF16)

    def remote(src, dst, send, recv, peer):
        return pltpu.make_async_remote_copy(
            src_ref=src, dst_ref=dst, send_sem=send, recv_sem=recv, device_id=peer, device_id_type=MESH
        )

    loads[0].wait()
    tp_tx[...] = jnp.dot(gated[...], wout[:, other_cols], preferred_element_type=F32).astype(BF16)
    own_mix = jnp.dot(gated[...], wout[:, mine_cols], preferred_element_type=F32).astype(BF16)
    pl.semaphore_wait(barrier, len(peers))
    swap = remote(tp_tx, tp_rx, tp_s, tp_r, partner)
    swap.start()
    base = hidden[...].astype(F32)
    swap.wait()
    mixed = own_mix.astype(F32) + tp_rx[...].astype(F32)
    resid = (base + mixed).astype(BF16)
    tokens[z, :, :half] = resid

    def block(origin):
        return tokens.at[(origin + nz) % nz]

    copies, arrivals = [], []
    for d in z_steps:
        q = len(copies)
        copies.append(remote(block(z), block(z), z_s.at[q], z_r.at[q], along_z(d)))
        arrivals.append(remote(block(z - d), block(z - d), z_s.at[q], z_r.at[q], along_z(d)))
        copies[q].start()
    far_up, far_down = nz // 2 - REACH, nz - 1 - nz // 2 - REACH
    for sign, count in ((1, far_up), (-1, far_down)):
        arrivals[0 if sign == 1 else 1].wait_recv()
        for hop in range(count, 0, -1):
            q = len(copies)
            origin, there = z - sign * REACH, z - sign * (REACH + hop)
            copies.append(remote(block(origin), block(origin), z_s.at[q], z_r.at[q], along_z(sign * hop)))
            arrivals.append(remote(block(there), block(there), z_s.at[q], z_r.at[q], along_z(sign * hop)))
            copies[q].start()
    for q in range(2, len(copies)):
        arrivals[q].wait_recv()

    held = tokens[...].astype(F32).reshape(nz * seqs, half + LANES)
    info = held[:, half:]
    info = info + jnp.where(iota(info.shape, 1) < TOPK, 0.0, pltpu.roll(info, LANES - TOPK, 1))
    row_z = iota((nz * seqs, rows), 0) // seqs
    col = iota((nz * seqs, rows), 1)
    slot_of = ((z * X_SIDE + col // slots) * CAP + col % CAP).astype(F32)
    same_z = (col % slots) // CAP == row_z
    takes = jnp.zeros((nz * seqs, rows), F32)
    mixing = jnp.zeros((nz * seqs, rows), F32)
    for i in range(TOPK):
        hit = same_z & (info[:, i : i + 1] == slot_of)
        takes = jnp.where(hit, 1.0, takes)
        mixing = jnp.where(hit, info[:, TOPK + i : TOPK + i + 1], mixing)
    mix_hi = mixing.astype(BF16)
    mix_lo = (mixing - mix_hi.astype(F32)).astype(BF16)
    picked = jnp.dot(takes.T.astype(BF16), held[:, :half].astype(BF16), preferred_element_type=F32).astype(BF16)
    pick_tx[...] = picked.reshape(X_SIDE, slots, half)

    def at_x(ref, d):
        return ref.at[(x + d + X_SIDE) % X_SIDE]

    order = [2, 1, 3]
    sent = []
    for i, d in enumerate(order):
        sent.append(remote(at_x(pick_tx, d), pick_rx.at[x], x_s.at[i], x_r.at[i], along_x(d)))
        sent[i].start()
    pick_rx[x] = pick_tx[x]
    shared = [remote(pick_tx.at[x], pick_other.at[x], o_s.at[3], o_r.at[3], partner)]
    shared[0].start()
    for i in (1, 2, 0):
        d = order[i]
        got = at_x(pick_rx, -d)
        remote(got, got, x_s.at[i], x_r.at[i], along_x(d)).wait_recv()
        shared.append(remote(got, at_x(pick_other, -d), o_s.at[i], o_r.at[i], partner))
        shared[-1].start()

    def project(values, cols):
        f = values[...].reshape(rows, half).astype(F32)
        scaled = (f * norm[0:1, cols].astype(F32)).astype(BF16)
        dims = (((1,), (1,)), ((), ()))
        g = lax.dot_general(scaled, wg[:, cols], dims, preferred_element_type=F32)
        u = lax.dot_general(scaled, wu[:, cols], dims, preferred_element_type=F32)
        return g, u, jnp.sum(f * f, axis=1, keepdims=True)

    for load in loads[1:]:
        load.wait()
    g0, u0, s0 = project(pick_rx, mine_cols)
    for copy in shared:
        copy.wait_recv()
    g1, u1, s1 = project(pick_other, other_cols)
    inv = lax.rsqrt((s0 + s1) / (2 * half) + EPSILON)
    act = (silu(inv * (g0 + g1)) * (inv * (u0 + u1))).astype(BF16)
    down_tx[...] = jnp.dot(act, wd[:, other_cols], preferred_element_type=F32).astype(BF16)
    trade = remote(down_tx, down_rx, d_s, d_r, partner)
    trade.start()
    own_down = jnp.dot(act, wd[:, mine_cols], preferred_element_type=F32).astype(BF16)
    trade.wait_recv()
    result = (own_down.astype(F32) + down_rx[...].astype(F32)).astype(BF16)
    back_tx[...] = result.reshape(X_SIDE, slots, half)

    returned = []
    for i, d in enumerate(order):
        returned.append(remote(at_x(back_tx, d), back_rx.at[x], b_s.at[i], b_r.at[i], along_x(d)))
        returned[i].start()
    back_rx[x] = back_tx[x]
    for i, d in enumerate(order):
        got = at_x(back_rx, -d)
        remote(got, got, b_s.at[i], b_r.at[i], along_x(d)).wait_recv()
    rows_back = back_rx[...].reshape(rows, half)
    part = jnp.dot(mix_hi, rows_back, preferred_element_type=F32) + jnp.dot(mix_lo, rows_back, preferred_element_type=F32)
    part = part.reshape(nz, seqs, half)
    sums[...] = part
    sums_bf[...] = part.astype(BF16)

    def at_z(ref, d):
        return ref.at[(z + d + nz) % nz]

    parts = []

    def send(src, dst, peer):
        q = len(parts)
        parts.append(remote(src, dst, h_s.at[q], h_r.at[q], peer))
        parts[q].start()

    for sign, count, first in ((1, far_up, 0), (-1, far_down, far_up)):
        for hop in range(count, 0, -1):
            send(at_z(sums_bf, -sign * (REACH + hop)), relay_rx.at[first + hop - 1], along_z(-sign * hop))
    near = [d for d in z_steps if abs(d) < REACH]
    for i, d in enumerate(near):
        send(at_z(sums_bf, -d), last_rx.at[i], along_z(-d))
    for n, (sign, count, first) in enumerate(((1, far_up, 0), (-1, far_down, far_up))):
        total = at_z(sums, -sign * REACH)[...]
        for hop in range(count, 0, -1):
            parts[first + count - hop].wait_recv()
            total = total + relay_rx[first + hop - 1].astype(F32)
        relay_tx[n] = total.astype(BF16)
        send(relay_tx.at[n], last_rx.at[len(near) + n], along_z(-sign * REACH))
    total = resid.astype(F32) + at_z(sums, 0)[...]
    for i in range(len(near) + 2):
        parts[far_up + far_down + i].wait_recv()
        total = total + last_rx[i].astype(F32)
    out[...] = total.astype(BF16)

    swap_done = [*copies, *sent, *shared, trade, *returned, *parts]
    for copy in swap_done:
        copy.wait_send()


def experts(ep, gated, hidden, wout, norm, chosen, weights, wg, wu, wd):
    seqs, half = hidden.shape
    nz = ep // X_SIDE
    slots = nz * CAP
    rows = X_SIDE * slots
    vmem = pl.BlockSpec(memory_space=pltpu.VMEM)
    hbm = pl.BlockSpec(memory_space=pl.ANY)
    dma = pltpu.SemaphoreType.DMA
    one = dma(())
    far = nz - 1 - 2 * REACH
    return pl.pallas_call(
        expert_kernel,
        name="experts",
        in_specs=[vmem, vmem, hbm, vmem, vmem, vmem, hbm, hbm, hbm],
        out_specs=vmem,
        out_shape=jax.ShapeDtypeStruct(hidden.shape, BF16),
        scratch_shapes=[
            pltpu.VMEM(wout.shape, BF16),
            pltpu.VMEM(wg.shape[1:], BF16),
            pltpu.VMEM(wu.shape[1:], BF16),
            pltpu.VMEM(wd.shape[1:], BF16),
            pltpu.VMEM((seqs, half), BF16),
            pltpu.VMEM((seqs, half), BF16),
            pltpu.VMEM((nz, seqs, half + LANES), BF16),
            pltpu.VMEM((X_SIDE, slots, half), BF16),
            pltpu.VMEM((X_SIDE, slots, half), BF16),
            pltpu.VMEM((X_SIDE, slots, half), BF16),
            pltpu.VMEM((rows, half), BF16),
            pltpu.VMEM((rows, half), BF16),
            pltpu.VMEM((X_SIDE, slots, half), BF16),
            pltpu.VMEM((X_SIDE, slots, half), BF16),
            pltpu.VMEM((nz, seqs, half), F32),
            pltpu.VMEM((nz, seqs, half), BF16),
            pltpu.VMEM((far, seqs, half), BF16),
            pltpu.VMEM((2, seqs, half), BF16),
            pltpu.VMEM((2 * REACH, seqs, half), BF16),
            dma((4,)), one, one, dma((nz - 1,)), dma((nz - 1,)), dma((3,)), dma((3,)), dma((4,)), dma((4,)),
            one, one, dma((3,)), dma((3,)), dma((nz - 1,)), dma((nz - 1,)),
        ],
        compiler_params=pltpu.CompilerParams(
            collective_id=0, has_side_effects=True, vmem_limit_bytes=40 * 1024 * 1024
        ),
    )(gated, hidden, wout, norm, chosen, weights, wg, wu, wd)


def on_device(
    ep,
    hidden,
    head_input_projected,
    output_gate_projected,
    input_map_projected,
    output_map_projected,
    raw_step_size,
    convolution_history,
    convolution_kernel,
    recurrent_state_matrix,
    head_decay_rate,
    extra_log_decay,
    head_skip_weight,
    output_matrix,
    expert_norm_scale,
    token_expert_index,
    token_expert_weight,
    expert_gate_weight,
    expert_up_weight,
    expert_down_weight,
):
    new_state, new_hist, gated = mixer(
        head_input_projected,
        output_gate_projected,
        input_map_projected,
        output_map_projected,
        raw_step_size,
        jnp.swapaxes(convolution_history, 0, 1),
        convolution_kernel,
        recurrent_state_matrix,
        head_decay_rate,
        extra_log_decay,
        head_skip_weight,
    )
    layer_out = experts(
        ep,
        gated,
        hidden,
        output_matrix,
        expert_norm_scale[None, :],
        token_expert_index,
        token_expert_weight,
        jnp.swapaxes(expert_gate_weight, 1, 2),
        jnp.swapaxes(expert_up_weight, 1, 2),
        expert_down_weight,
    )
    return (layer_out, new_state, jnp.swapaxes(new_hist, 0, 1))


def solution(mesh):
    in_specs = (
        P(("grp", "ep"), "tp"),
        P(("grp", "ep"), "tp"),
        P(("grp", "ep"), "tp"),
        P(("grp", "ep"), "tp"),
        P(("grp", "ep"), "tp"),
        P(("grp", "ep"), "tp"),
        P(("grp", "ep"), None, "tp"),
        P(None, "tp"),
        P(("grp", "ep"), "tp", None, None),
        P("tp"),
        P(("grp", "ep"), "tp"),
        P("tp"),
        P("tp", None),
        P(),
        P(("grp", "ep"), None),
        P(("grp", "ep"), None),
        P("ep", None, "tp"),
        P("ep", None, "tp"),
        P("ep", "tp", None),
    )
    out_specs = (
        P(("grp", "ep"), "tp"),
        P(("grp", "ep"), "tp", None, None),
        P(("grp", "ep"), None, "tp"),
    )
    return jax.shard_map(
        functools.partial(on_device, mesh.shape["ep"]),
        mesh=mesh,
        in_specs=in_specs,
        out_specs=out_specs,
        check_vma=False,
    )
```

time: 115 us -> 78.5 us (0.68)
  Pallas kernels: 0 us -> 71.6 us
  waiting for transfers between devices: 43.1 us -> 0 us
  starting transfers between devices: 38.8 us -> 0 us
  matrix products: 9.8 us -> 0 us
  other arithmetic: 8.23 us -> 0 us
  blocking collectives: 6.58 us -> 0 us
    pallas_call x0 -> x2, Pallas kernels: none -> 71.6 us  [the longest x1 63.2 us: experts(): pl.pallas_call(expert_kernel, name='experts', in_specs=[vmem, vmem, hbm,...]
    all_to_all x3 -> x0, waiting for transfers between devices: 43.1 us -> none  [the longest x1 21.5 us: on_device(): lax.all_to_all(outgoing.reshape(ep_count, capacity, half_width), 'ep', sp...]
    all_to_all x3 -> x0, starting transfers between devices: 38.8 us -> none  [the longest x1 29 us: on_device(): lax.all_to_all(outgoing.reshape(ep_count, capacity, half_width), 'ep', sp...]
    dot_general x6 -> x0, matrix products: 9.8 us -> none  [the longest x1 3.55 us: on_device(): jnp.dot(gated, output_matrix, preferred_element_type=jnp.float32)]
    reshape x8 -> x0, local copies, waits for them, and re-layouts: 4.22 us -> none  [the longest x1 0.87 us: on_device(): input_map_projected.astype(jnp.float32)]
    all_to_all x1 -> x0, blocking collectives: 4.17 us -> none  [sent_and_summed(): lax.all_to_all(pieces, axis, split_axis=0, concat_axis=0, tiled=True)]
    add x3 -> x0, other arithmetic: 3.86 us -> none  [the longest x1 3.76 us: on_device(): decay_factor[:, :, None, None] * recurrent_state_matrix]
    unnamed x23 -> x17, local copies, waits for them, and re-layouts: 2.1 us -> 4.89 us
  transfers between devices with their start and end apart: 3 -> 0, of which waited for: 3 -> 0; matrix products, arithmetic and copies ran while one was open for 1% -> 0% of each run, Pallas kernels for 0% -> 0%
where the time goes in v1:
time: 78.5 us; the launch traced here: 78.1 us
  Pallas kernels  71.6 us (91%)
  local copies, waits for them, and re-layouts  5.73 us (7%)
    pallas_call x1, Pallas kernels, experts(): pl.pallas_call(expert_kernel, name='experts', in_specs=[vmem, vmem, hbm,...  63.2 us
    pallas_call x1, Pallas kernels, mixer(): pl.pallas_call(mixer_kernel, name='mixer', grid=(seqs,), in_specs=[whole(...  8.44 us
    unnamed x17, local copies, waits for them, and re-layouts  4.89 us

profile of v1, /device:TPU:40, one launch (start us, length us, event | category | flops | bytes accessed | tf_op | source)
XLA Modules:
  0.0 78.1 jit_solution(14847583747863525066)
XLA Ops:
  0.6 0.0 copy-start.2
  0.6 0.0 copy-start.1
  0.7 0.0 copy-start.7
  0.7 0.0 copy-start.6
  0.7 0.0 copy-start.4
  0.7 0.8 %broadcast_in_dim.3.norm = bf16[1,2048]{1,0:T(2,128)(2,1)S(1)} reshape(bf16[2048]{0:T(1024)(128)(2,1)} %param.32) | data formatting | bytes 8192 | tf_op jit(solution)/shard_map/broadcast_in_dim | solution.py:425
  1.5 8.4 %mixer.1 = (f32[8,16,64,64]{3,2,1,0:T(8,128)}, bf16[3,8,1024]{2,1,0:T(8,128)(2,1)}, bf16[8,1024]{1,0:T(8,128)(2,1)}) custom-call(bf16[8,1024]{1,0:T(8,128)(2,1)} %head_in.1, bf16[8,1024]{1,0:T(8,128)(2,1)} %gate.1, bf16[8,128]{1,0:T(8,128)(2,1)} %b_map.1, bf16[8,128]{1,0:T(8,128)(2,1)} %c_map.1, bf16[8,16]{1,0:T(8,128)(2,1)} %raw_step.1, ...), custom_call_target="tpu_custom_call" | custom-call | tf_op jit(solution)/shard_map/mixer/pallas_call | solution.py:112
  10.0 0.0 copy-done.2
  10.0 0.0 copy-done.1
  10.0 0.0 copy-done.7
  10.0 0.0 copy-done.6
  10.0 0.0 copy-done.4
  10.0 0.0 copy-start
  10.0 2.2 %copy-done = bf16[1024,2048]{1,0:T(8,128)(2,1)S(1)} copy-done((bf16[1024,2048]{1,0:T(8,128)(2,1)S(1)}, bf16[1024,2048]{1,0:T(8,128)(2,1)}, u32[]{:S(2)}) %copy-start) | copy-done | bytes 4194328
  12.2 0.0 copy-start.3
  12.2 1.4 %copy-done.3 = bf16[1,352,2048]{2,1,0:T(8,128)(2,1)S(1)} copy-done((bf16[1,352,2048]{2,1,0:T(8,128)(2,1)S(1)}, bf16[1,352,2048]{2,1,0:T(8,128)(2,1)}, u32[]{:S(2)}) %copy-start.3) | copy-done | bytes 1441816
  13.6 0.0 copy-start.5
  13.6 0.7 copy-done.5
  14.3 63.2 %experts.1 = bf16[8,1024]{1,0:T(8,128)(2,1)S(1)} custom-call(bf16[8,1024]{1,0:T(8,128)(2,1)S(1)} %copy-done.5, bf16[8,1024]{1,0:T(8,128)(2,1)S(1)} %copy-done.4, bf16[1024,2048]{1,0:T(8,128)(2,1)S(1)} %copy-done, bf16[1,2048]{1,0:T(2,128)(2,1)S(1)} %broadcast_in_dim.3.norm, s32[8,6]{1,0:T(8,128)S(1)} %copy-done.6, f32[8,6]{1,0:T(8,128)S(1)} %copy-done.7, ...), custom_call_target="tpu_custom_call" | custom-call | tf_op jit(solution)/shard_map/experts/pallas_call | solution.py:350
  77.5 0.6 copy.23
Async XLA Ops:
  0.6 9.3 %copy-start.2 = (bf16[1,2048,352]{1,2,0:T(8,128)(2,1)S(1)}, bf16[1,2048,352]{1,2,0:T(8,128)(2,1)}, u32[]{:S(2)}) copy-start(bf16[1,2048,352]{1,2,0:T(8,128)(2,1)} %param.36) | copy-start | bytes 4325380
  0.6 9.3 %copy-start.1 = (bf16[1,2048,352]{1,2,0:T(8,128)(2,1)S(1)}, bf16[1,2048,352]{1,2,0:T(8,128)(2,1)}, u32[]{:S(2)}) copy-start(bf16[1,2048,352]{1,2,0:T(8,128)(2,1)} %param.35) | copy-start | bytes 4325380
  0.7 9.3 %copy-start.7 = (f32[8,6]{1,0:T(8,128)S(1)}, f32[8,6]{1,0:T(8,128)}, u32[]{:S(2)}) copy-start(f32[8,6]{1,0:T(8,128)} %weights.1) | copy-start | bytes 580
  0.7 9.3 %copy-start.6 = (s32[8,6]{1,0:T(8,128)S(1)}, s32[8,6]{1,0:T(8,128)}, u32[]{:S(2)}) copy-start(s32[8,6]{1,0:T(8,128)} %chosen.1) | copy-start | bytes 580
  0.7 9.3 %copy-start.4 = (bf16[8,1024]{1,0:T(8,128)(2,1)S(1)}, bf16[8,1024]{1,0:T(8,128)(2,1)}, u32[]{:S(2)}) copy-start(bf16[8,1024]{1,0:T(8,128)(2,1)} %hidden.1) | copy-start | bytes 49156
  10.0 2.2 %copy-start = (bf16[1024,2048]{1,0:T(8,128)(2,1)S(1)}, bf16[1024,2048]{1,0:T(8,128)(2,1)}, u32[]{:S(2)}) copy-start(bf16[1024,2048]{1,0:T(8,128)(2,1)} %wout_h.1) | copy-start | bytes 12582916
  12.2 1.4 %copy-start.3 = (bf16[1,352,2048]{2,1,0:T(8,128)(2,1)S(1)}, bf16[1,352,2048]{2,1,0:T(8,128)(2,1)}, u32[]{:S(2)}) copy-start(bf16[1,352,2048]{2,1,0:T(8,128)(2,1)} %wd_h.1) | copy-start | bytes 4325380
  13.6 0.7 copy-start.5

commit v2 on v1

v2 whole, which is shorter than its diff:
```python
import functools

import jax
import jax.numpy as jnp
from jax import lax
from jax.experimental import pallas as pl
from jax.experimental.pallas import tpu as pltpu
from jax.sharding import PartitionSpec as P

MESH = pl.DeviceIdType.MESH
F32 = jnp.float32
BF16 = jnp.bfloat16

STATE_DIM = 64
TOPK = 6
CAP = 2
EPSILON = 1e-06
X_SIDE = 4
FIRST = [(0, (5, -5, 2, -2, 1, -1))]
FAN = [(5, (3, 2, -2, 1, -1)), (11, (-2, 2, -1, 1))]
LANES = 128
HIGH = lax.Precision.HIGHEST
VMEM_BYTES = 28 * 1024 * 1024


def iota(shape, dim):
    return lax.broadcasted_iota(jnp.int32, shape, dim)


def silu(v):
    return v / (1.0 + jnp.exp(-v))


def softplus(v):
    return jnp.maximum(v, 0.0) + jnp.log1p(jnp.exp(-jnp.abs(v)))


def layer_kernel(
    hidden_h, head_in_h, gate_h, b_map_h, c_map_h, raw_step_h, hist_h, taps_h, state_h, rate_h, extra_h, skip_h, wout_h,
    norm_h, chosen_h, weights_h, wg_h, wu_h, wd_h,
    out, new_state, new_hist,
    hidden, head_in, gate, b_map, c_map, raw_step, hist, taps, state, rate, extra_decay, skip, wout,
    norm, chosen, weights, wg, wu, wd,
    tp_tx, tp_rx, tokens, pick_tx, pick_rx, pick_other, down_tx, down_rx, back_tx, back_rx,
    sums, sums_bf, relay_rx, relay_tx, last_rx,
    in_sem, w_sem, tp_s, tp_r, z_s, z_r, x_s, x_r, o_s, o_r, d_s, d_r, b_s, b_r, h_s, h_r,
):
    seqs, half = hidden.shape
    nz = tokens.shape[0]
    slots = nz * CAP
    rows = X_SIDE * slots
    me, core = lax.axis_index("ep"), lax.axis_index("tp")
    z, x = me // X_SIDE, me % X_SIDE
    other = 1 - core

    def along_z(d):
        return {"ep": ((z + d + nz) % nz) * X_SIDE + x}

    def along_x(d):
        return {"ep": z * X_SIDE + (x + d) % X_SIDE}

    partner = {"tp": other}
    mine_cols = pl.ds(pl.multiple_of(core * half, half), half)
    other_cols = pl.ds(pl.multiple_of(other * half, half), half)

    barrier = pltpu.get_barrier_semaphore()
    steps = sorted({s * h for _, hops in FIRST + FAN for h in hops for s in (1, -1)})
    peers = [along_z(h) for h in steps] + [along_x(d) for d in range(1, X_SIDE)] + [partner]
    for peer in peers:
        pl.semaphore_signal(barrier, inc=1, device_id=peer, device_id_type=MESH)
    pairs = [(head_in_h, head_in), (hist_h, hist), (taps_h, taps), (raw_step_h, raw_step), (extra_h, extra_decay), (rate_h, rate),
             (skip_h, skip), (b_map_h, b_map), (c_map_h, c_map), (gate_h, gate), (hidden_h, hidden), (chosen_h, chosen),
             (weights_h, weights), (norm_h, norm)]
    small = [pltpu.make_async_copy(src, dst, in_sem.at[i]) for i, (src, dst) in enumerate(pairs)]
    for copy in small:
        copy.start()
    fetch = [pltpu.make_async_copy(state_h.at[s], state.at[s], in_sem.at[len(pairs) + s]) for s in range(seqs)]
    for copy in fetch:
        copy.start()
    get_wout = pltpu.make_async_copy(wout_h, wout, w_sem.at[0])
    loads = [pltpu.make_async_copy(src, dst, w_sem.at[1 + i])
             for i, (src, dst) in enumerate([(wg_h.at[0], wg), (wu_h.at[0], wu), (wd_h.at[0], wd)])]
    for copy in small:
        copy.wait()

    heads = raw_step.shape[1]
    width = half // heads
    groups = b_map.shape[1] // STATE_DIM
    per_group = heads // groups
    chans = per_group * width
    fresh_in = head_in[...]
    for i in range(2):
        new_hist[i] = hist[i + 1]
    new_hist[2] = fresh_in
    kern = taps[...].astype(F32)
    total = fresh_in.astype(F32) * kern[3:4]
    for i in range(3):
        total = total + hist[i].astype(F32) * kern[i : i + 1]
    conv = silu(total)
    dt = softplus(raw_step[...].astype(F32))
    col = iota((seqs, heads), 1)
    rates = jnp.zeros((seqs, heads), F32)
    for h in range(heads):
        rates = jnp.where(col == h, rate[h], rates)
    decay = jnp.exp(-rates * dt + extra_decay[...])
    lanes_of = (iota((heads, half), 1) // width == iota((heads, half), 0)).astype(F32)
    spread = jnp.dot(jnp.concatenate([dt, decay], axis=0), lanes_of, precision=HIGH, preferred_element_type=F32)
    u = conv * spread[:seqs]
    decays = spread[seqs:]
    col = iota((seqs, half), 1) // width
    skips = jnp.zeros((seqs, half), F32)
    for h in range(heads):
        skips = jnp.where(col == h, skip[h], skips)
    opened = silu(gate[...].astype(F32))
    b_all = b_map[...].astype(F32)
    c_all = c_map[...].astype(F32)

    row_c = iota((seqs, STATE_DIM), 0)
    read = []
    for g in range(groups):
        cols = slice(g * STATE_DIM, (g + 1) * STATE_DIM)
        read.append(u[:, g * chans : (g + 1) * chans] * jnp.sum(b_all[:, cols] * c_all[:, cols], axis=1, keepdims=True))
    seen = [jnp.zeros((seqs, chans), F32) for _ in range(groups)]
    for s in range(seqs):
        fetch[s].wait()
        if s == seqs // 2:
            get_wout.start()
        for g in range(groups):
            c_g = jnp.where(row_c == s, c_all[:, g * STATE_DIM : (g + 1) * STATE_DIM], 0.0).astype(BF16)
            held = state[s, g * per_group : (g + 1) * per_group].reshape(chans, STATE_DIM).astype(BF16)
            seen[g] = seen[g] + lax.dot_general(c_g, held, (((1,), (1,)), ((), ())), preferred_element_type=F32)
    for load in loads:
        load.start()
    readout = decays * jnp.concatenate(seen, axis=1) + jnp.concatenate(read, axis=1) + skips * conv
    gated = (readout * opened).astype(BF16)

    idx = chosen[...]
    wts = weights[...]
    lane = iota((seqs, LANES), 1)
    named = jnp.zeros((seqs, LANES), F32)
    for i in range(TOPK):
        named = named + (lane == idx[:, i : i + 1]).astype(F32)
    before = (iota((seqs, seqs), 1) < iota((seqs, seqs), 0)).astype(BF16)
    rank = jnp.dot(before, named.astype(BF16), preferred_element_type=F32)
    extra = jnp.zeros((seqs, LANES), F32)
    for i in range(TOPK):
        expert = idx[:, i : i + 1]
        place = jnp.sum(jnp.where(lane == expert, rank, 0.0), axis=1, keepdims=True)
        slot = expert.astype(F32) * CAP + place
        w = wts[:, i : i + 1]
        w_hi = w.astype(BF16).astype(F32)
        extra = jnp.where(lane == i, slot, extra)
        extra = jnp.where(lane == TOPK + i, w_hi, extra)
        extra = jnp.where(lane == 2 * TOPK + i, w - w_hi, extra)
    tokens[0, :, half:] = extra.astype(BF16)

    def remote(src, dst, send, recv, peer):
        return pltpu.make_async_remote_copy(
            src_ref=src, dst_ref=dst, send_sem=send, recv_sem=recv, device_id=peer, device_id_type=MESH
        )

    get_wout.wait()
    tp_tx[...] = jnp.dot(gated, wout[:, other_cols], preferred_element_type=F32).astype(BF16)
    pl.semaphore_wait(barrier, len(peers))
    swap = remote(tp_tx, tp_rx, tp_s, tp_r, partner)
    swap.start()
    own_mix = jnp.dot(gated, wout[:, mine_cols], preferred_element_type=F32).astype(BF16)
    base = hidden[...].astype(F32)
    swap.wait()
    mixed = own_mix.astype(F32) + tp_rx[...].astype(F32)
    resid = (base + mixed).astype(BF16)
    tokens[0, :, :half] = resid

    def update_states():
        u_hi = u.astype(BF16).astype(F32)
        u_t = jnp.concatenate([u_hi, u - u_hi], axis=0).T.astype(BF16)
        row = iota((2 * seqs, STATE_DIM), 0)
        for s in range(seqs):
            for g in range(groups):
                b_g = b_all[:, g * STATE_DIM : (g + 1) * STATE_DIM]
                b_g = jnp.where(row % seqs == s, jnp.concatenate([b_g, b_g], axis=0), 0.0).astype(BF16)
                outer = jnp.dot(u_t[g * chans : (g + 1) * chans], b_g, preferred_element_type=F32)
                for j in range(per_group):
                    h = g * per_group + j
                    new_state[s, h] = decay[s : s + 1, h : h + 1] * state[s, h] + outer[j * width : (j + 1) * width]

    copies, arrived = [], {}
    for origin, hops in FIRST + FAN:
        if origin == FAN[0][0]:
            update_states()
        if origin:
            arrived.pop(origin).wait_recv()
        for hop in hops:
            q = len(copies)
            lands = (origin + hop) % nz
            copies.append(remote(tokens.at[origin], tokens.at[lands], z_s.at[q], z_r.at[q], along_z(hop)))
            arrived[lands] = copies[q]
            copies[q].start()
    for copy in arrived.values():
        copy.wait_recv()

    held = tokens[...].astype(F32).reshape(nz * seqs, half + LANES)
    info = held[:, half:]
    info = info + jnp.where(iota(info.shape, 1) < TOPK, 0.0, pltpu.roll(info, LANES - TOPK, 1))
    row_z = iota((nz * seqs, rows), 0) // seqs
    col = iota((nz * seqs, rows), 1)
    slot_of = ((z * X_SIDE + col // slots) * CAP + col % CAP).astype(F32)
    same_z = (col % slots) // CAP == row_z
    takes = jnp.zeros((nz * seqs, rows), F32)
    mixing = jnp.zeros((nz * seqs, rows), F32)
    for i in range(TOPK):
        hit = same_z & (info[:, i : i + 1] == slot_of)
        takes = jnp.where(hit, 1.0, takes)
        mixing = jnp.where(hit, info[:, TOPK + i : TOPK + i + 1], mixing)
    mix_hi = mixing.astype(BF16)
    mix_lo = (mixing - mix_hi.astype(F32)).astype(BF16)
    picked = jnp.dot(takes.T.astype(BF16), held[:, :half].astype(BF16), preferred_element_type=F32).astype(BF16)
    pick_tx[...] = picked.reshape(X_SIDE, slots, half)

    def at_x(ref, d):
        return ref.at[(x + d + X_SIDE) % X_SIDE]

    order = [2, 1, 3]
    sent = []
    for i, d in enumerate(order):
        sent.append(remote(at_x(pick_tx, d), pick_rx.at[x], x_s.at[i], x_r.at[i], along_x(d)))
        sent[i].start()
    pick_rx[x] = pick_tx[x]
    shared = [remote(pick_tx.at[x], pick_other.at[x], o_s.at[3], o_r.at[3], partner)]
    shared[0].start()
    for i in (1, 2, 0):
        d = order[i]
        got = at_x(pick_rx, -d)
        remote(got, got, x_s.at[i], x_r.at[i], along_x(d)).wait_recv()
        shared.append(remote(got, at_x(pick_other, -d), o_s.at[i], o_r.at[i], partner))
        shared[-1].start()

    def project(values, cols):
        f = values[...].reshape(rows, half).astype(F32)
        scaled = (f * norm[cols].astype(F32)[None, :]).astype(BF16)
        dims = (((1,), (1,)), ((), ()))
        g = lax.dot_general(scaled, wg[:, cols], dims, preferred_element_type=F32)
        u = lax.dot_general(scaled, wu[:, cols], dims, preferred_element_type=F32)
        return g, u, jnp.sum(f * f, axis=1, keepdims=True)

    for load in loads:
        load.wait()
    g0, u0, s0 = project(pick_rx, mine_cols)
    for copy in shared:
        copy.wait_recv()
    g1, u1, s1 = project(pick_other, other_cols)
    inv = lax.rsqrt((s0 + s1) / (2 * half) + EPSILON)
    act = (silu(inv * (g0 + g1)) * (inv * (u0 + u1))).astype(BF16)
    down_tx[...] = jnp.dot(act, wd[:, other_cols], preferred_element_type=F32).astype(BF16)
    trade = remote(down_tx, down_rx, d_s, d_r, partner)
    trade.start()
    own_down = jnp.dot(act, wd[:, mine_cols], preferred_element_type=F32).astype(BF16)
    trade.wait_recv()
    result = (own_down.astype(F32) + down_rx[...].astype(F32)).astype(BF16)
    back_tx[...] = result.reshape(X_SIDE, slots, half)

    returned = []
    for i, d in enumerate(order):
        returned.append(remote(at_x(back_tx, d), back_rx.at[x], b_s.at[i], b_r.at[i], along_x(d)))
        returned[i].start()
    back_rx[x] = back_tx[x]
    for i, d in enumerate(order):
        got = at_x(back_rx, -d)
        remote(got, got, b_s.at[i], b_r.at[i], along_x(d)).wait_recv()
    rows_back = back_rx[...].reshape(rows, half)
    part = jnp.dot(mix_hi, rows_back, preferred_element_type=F32) + jnp.dot(mix_lo, rows_back, preferred_element_type=F32)
    part = part.reshape(nz, seqs, half)
    sums[...] = part
    sums_bf[...] = part.astype(BF16)

    parts = []

    def send(src, dst, hop):
        q = len(parts)
        parts.append(remote(src, dst, h_s.at[q], h_r.at[q], along_z(hop)))
        parts[q].start()
        return parts[q]

    gathered = {}
    n = 0
    for origin, hops in FAN:
        for hop in hops:
            gathered.setdefault(origin, []).append((send(sums_bf.at[(origin + hop) % nz], relay_rx.at[n], -hop), n))
            n += 1
    finals = []
    (_, first_hops), = FIRST
    for hop in first_hops[len(FAN):]:
        finals.append(send(sums_bf.at[hop % nz], last_rx.at[len(finals)], -hop))
    for i, (origin, _) in enumerate(FAN):
        total = sums[origin]
        for copy, at in gathered[origin]:
            copy.wait_recv()
            total = total + relay_rx[at].astype(F32)
        relay_tx[i] = total.astype(BF16)
        finals.append(send(relay_tx.at[i], last_rx.at[len(finals)], -first_hops[i]))
    total = resid.astype(F32) + sums[0]
    for i, copy in enumerate(finals):
        copy.wait_recv()
        total = total + last_rx[i].astype(F32)
    out[...] = total.astype(BF16)

    swap_done = [*copies, *sent, *shared, trade, *returned, *parts]
    for copy in swap_done:
        copy.wait_send()


def layer(ep, *args):
    hidden, head_in, gate, b_map, c_map, raw_step, hist, taps, state, rate, extra, skip, wout, norm, chosen, weights, wg, wu, wd = args
    seqs, half = hidden.shape
    nz = ep // X_SIDE
    slots = nz * CAP
    rows = X_SIDE * slots
    far = sum(len(hops) for _, hops in FAN)
    near = len(FIRST[0][1])
    vmem = pl.BlockSpec(memory_space=pltpu.VMEM)
    hbm = pl.BlockSpec(memory_space=pltpu.HBM)
    dma = pltpu.SemaphoreType.DMA
    one = dma(())

    def room(a):
        return pltpu.VMEM(a.shape, a.dtype)

    return pl.pallas_call(
        layer_kernel,
        name="layer",
        in_specs=[hbm] * len(args),
        out_specs=[vmem, vmem, vmem],
        out_shape=[
            pltpu.VMEM(hidden.shape, BF16),
            pltpu.VMEM(state.shape, F32),
            pltpu.VMEM(hist.shape, BF16),
        ],
        scratch_shapes=[
            *(pltpu.SMEM(a.shape, F32) if a is rate or a is skip else room(a) for a in args[:16]),
            *(pltpu.VMEM(a.shape[1:], BF16) for a in (wg, wu, wd)),
            room(hidden),
            room(hidden),
            pltpu.VMEM((nz, seqs, half + LANES), BF16),
            *(pltpu.VMEM((X_SIDE, slots, half), BF16) for _ in range(3)),
            *(pltpu.VMEM((rows, half), BF16) for _ in range(2)),
            *(pltpu.VMEM((X_SIDE, slots, half), BF16) for _ in range(2)),
            pltpu.VMEM((nz, seqs, half), F32),
            pltpu.VMEM((nz, seqs, half), BF16),
            pltpu.VMEM((far, seqs, half), BF16),
            pltpu.VMEM((2, seqs, half), BF16),
            pltpu.VMEM((near, seqs, half), BF16),
            dma((14 + seqs,)), dma((4,)), one, one, dma((nz - 1,)), dma((nz - 1,)), dma((3,)), dma((3,)), dma((4,)), dma((4,)),
            one, one, dma((3,)), dma((3,)), dma((nz - 1,)), dma((nz - 1,)),
        ],
        compiler_params=pltpu.CompilerParams(collective_id=0, has_side_effects=True, vmem_limit_bytes=VMEM_BYTES),
    )(*(pltpu.with_memory_space_constraint(a, pltpu.HBM) for a in args))


def store_kernel(*refs):
    count = (len(refs) - 1) // 2
    sem = refs[-1]
    copies = [pltpu.make_async_copy(refs[i], refs[count + i], sem.at[i]) for i in range(count)]
    for copy in copies:
        copy.start()
    for copy in copies:
        copy.wait()


def store(*values):
    return pl.pallas_call(
        store_kernel,
        name="store",
        in_specs=[pl.BlockSpec(memory_space=pltpu.VMEM)] * len(values),
        out_specs=[pl.BlockSpec(memory_space=pltpu.HBM)] * len(values),
        out_shape=[pltpu.HBM(v.shape, v.dtype) for v in values],
        scratch_shapes=[pltpu.SemaphoreType.DMA((len(values),))],
        compiler_params=pltpu.CompilerParams(vmem_limit_bytes=VMEM_BYTES),
    )(*(pltpu.with_memory_space_constraint(v, pltpu.VMEM) for v in values))


def on_device(
    ep,
    hidden,
    head_input_projected,
    output_gate_projected,
    input_map_projected,
    output_map_projected,
    raw_step_size,
    convolution_history,
    convolution_kernel,
    recurrent_state_matrix,
    head_decay_rate,
    extra_log_decay,
    head_skip_weight,
    output_matrix,
    expert_norm_scale,
    token_expert_index,
    token_expert_weight,
    expert_gate_weight,
    expert_up_weight,
    expert_down_weight,
):
    layer_out, new_state, new_hist = store(*layer(
        ep,
        hidden,
        head_input_projected,
        output_gate_projected,
        input_map_projected,
        output_map_projected,
        raw_step_size,
        jnp.swapaxes(convolution_history, 0, 1),
        convolution_kernel,
        recurrent_state_matrix,
        head_decay_rate,
        extra_log_decay,
        head_skip_weight,
        output_matrix,
        expert_norm_scale,
        token_expert_index,
        token_expert_weight,
        jnp.swapaxes(expert_gate_weight, 1, 2),
        jnp.swapaxes(expert_up_weight, 1, 2),
        expert_down_weight,
    ))
    return (layer_out, new_state, jnp.swapaxes(new_hist, 0, 1))


def solution(mesh):
    in_specs = (
        P(("grp", "ep"), "tp"),
        P(("grp", "ep"), "tp"),
        P(("grp", "ep"), "tp"),
        P(("grp", "ep"), "tp"),
        P(("grp", "ep"), "tp"),
        P(("grp", "ep"), "tp"),
        P(("grp", "ep"), None, "tp"),
        P(None, "tp"),
        P(("grp", "ep"), "tp", None, None),
        P("tp"),
        P(("grp", "ep"), "tp"),
        P("tp"),
        P("tp", None),
        P(),
        P(("grp", "ep"), None),
        P(("grp", "ep"), None),
        P("ep", None, "tp"),
        P("ep", None, "tp"),
        P("ep", "tp", None),
    )
    out_specs = (
        P(("grp", "ep"), "tp"),
        P(("grp", "ep"), "tp", None, None),
        P(("grp", "ep"), None, "tp"),
    )
    return jax.shard_map(
        functools.partial(on_device, mesh.shape["ep"]),
        mesh=mesh,
        in_specs=in_specs,
        out_specs=out_specs,
        check_vma=False,
    )
```

time: 78.5 us -> 66.2 us (0.84)
  Pallas kernels: 71.6 us -> 65.4 us
  local copies, waits for them, and re-layouts: 5.73 us -> 0 us
    pallas_call x2, Pallas kernels: 71.6 us -> 65.4 us  [the longest x1 63.3 us: layer(): pl.pallas_call(layer_kernel, name='layer', in_specs=[hbm] * len(args), ou...]
    unnamed x17 -> x0, local copies, waits for them, and re-layouts: 4.89 us -> none
    broadcast_in_dim x1 -> x0, local copies, waits for them, and re-layouts: 0.84 us -> none  [on_device(): expert_norm_scale[None, :]]
where the time goes in v2:
time: 66.2 us; the launch traced here: 66 us
  Pallas kernels  65.4 us (99%)
    pallas_call x1, Pallas kernels, layer(): pl.pallas_call(layer_kernel, name='layer', in_specs=[hbm] * len(args), ou...  63.3 us
    pallas_call x1, Pallas kernels, store(): pl.pallas_call(store_kernel, name='store', in_specs=[pl.BlockSpec(memory_...  2.05 us

profile of v2, /device:TPU:40, one launch (start us, length us, event | category | flops | bytes accessed | tf_op | source)
XLA Modules:
  0.0 66.0 jit_solution(6049974015280131790)
XLA Ops:
  0.6 63.3 %layer.1 = (bf16[8,1024]{1,0:T(8,128)(2,1)S(1)}, f32[8,16,64,64]{3,2,1,0:T(8,128)S(1)}, bf16[3,8,1024]{2,1,0:T(8,128)(2,1)S(1)}) custom-call(bf16[8,1024]{1,0:T(8,128)(2,1)} %hidden_h.1, bf16[8,1024]{1,0:T(8,128)(2,1)} %head_in_h.1, bf16[8,1024]{1,0:T(8,128)(2,1)} %gate_h.1, bf16[8,128]{1,0:T(8,128)(2,1)} %b_map_h.1, bf16[8,128]{1,0:T(8,128)(2,1)} %c_map_h.1, ...), custom_call_target="tpu_custom_call" | custom-call | tf_op jit(solution)/shard_map/layer/pallas_call | solution.py:328
  64.0 2.0 %store.1 = (bf16[8,1024]{1,0:T(8,128)(2,1)}, f32[8,16,64,64]{3,2,1,0:T(8,128)}, bf16[3,8,1024]{2,1,0:T(8,128)(2,1)}) custom-call(bf16[8,1024]{1,0:T(8,128)(2,1)S(1)} %get-tuple-element.9.refs_0_, f32[8,16,64,64]{3,2,1,0:T(8,128)S(1)} %get-tuple-element.10.refs_1_, bf16[3,8,1024]{2,1,0:T(8,128)(2,1)S(1)} %get-tuple-element.11.refs_2_), custom_call_target="tpu_custom_call" | custom-call | tf_op jit(solution)/shard_map/store/pallas_call | solution.py:370

commit v3 on v2

--- a/solution.py
+++ b/solution.py
@@ -16,8 +16,10 @@
 CAP = 2
 EPSILON = 1e-06
 X_SIDE = 4
-FIRST = [(0, (5, -5, 2, -2, 1, -1))]
-FAN = [(5, (3, 2, -2, 1, -1)), (11, (-2, 2, -1, 1))]
+FIRST = (5, -5, 2, -2, 1, -1)
+RELAYS = (5, 11)
+FAN = {5: (3, 2, -2, 1, -1), 11: (-2, 2, -1, 1)}
+ORDER = (2, 1, 3)
 LANES = 128
 HIGH = lax.Precision.HIGHEST
 VMEM_BYTES = 28 * 1024 * 1024
@@ -47,7 +49,8 @@
 ):
     seqs, half = hidden.shape
     nz = tokens.shape[0]
-    slots = nz * CAP
+    some = nz // 2
+    slots = some * CAP
     rows = X_SIDE * slots
     me, core = lax.axis_index("ep"), lax.axis_index("tp")
     z, x = me // X_SIDE, me % X_SIDE
@@ -64,7 +67,7 @@
     other_cols = pl.ds(pl.multiple_of(other * half, half), half)
 
     barrier = pltpu.get_barrier_semaphore()
-    steps = sorted({s * h for _, hops in FIRST + FAN for h in hops for s in (1, -1)})
+    steps = sorted({s * h for hops in (FIRST, *FAN.values()) for h in hops for s in (1, -1)})
     peers = [along_z(h) for h in steps] + [along_x(d) for d in range(1, X_SIDE)] + [partner]
     for peer in peers:
         pl.semaphore_signal(barrier, inc=1, device_id=peer, device_id_type=MESH)
@@ -78,6 +81,7 @@
     for copy in fetch:
         copy.start()
     get_wout = pltpu.make_async_copy(wout_h, wout, w_sem.at[0])
+    get_wout.start()
     loads = [pltpu.make_async_copy(src, dst, w_sem.at[1 + i])
              for i, (src, dst) in enumerate([(wg_h.at[0], wg), (wu_h.at[0], wu), (wd_h.at[0], wd)])]
     for copy in small:
@@ -123,8 +127,6 @@
     seen = [jnp.zeros((seqs, chans), F32) for _ in range(groups)]
     for s in range(seqs):
         fetch[s].wait()
-        if s == seqs // 2:
-            get_wout.start()
         for g in range(groups):
             c_g = jnp.where(row_c == s, c_all[:, g * STATE_DIM : (g + 1) * STATE_DIM], 0.0).astype(BF16)
             held = state[s, g * per_group : (g + 1) * per_group].reshape(chans, STATE_DIM).astype(BF16)
@@ -133,6 +135,18 @@
         load.start()
     readout = decays * jnp.concatenate(seen, axis=1) + jnp.concatenate(read, axis=1) + skips * conv
     gated = (readout * opened).astype(BF16)
+
+    def remote(src, dst, send, recv, peer):
+        return pltpu.make_async_remote_copy(
+            src_ref=src, dst_ref=dst, send_sem=send, recv_sem=recv, device_id=peer, device_id_type=MESH
+        )
+
+    get_wout.wait()
+    tp_tx[...] = jnp.dot(gated, wout[:, other_cols], preferred_element_type=F32).astype(BF16)
+    pl.semaphore_wait(barrier, len(peers))
+    swap = remote(tp_tx, tp_rx, tp_s, tp_r, partner)
+    swap.start()
+    own_mix = jnp.dot(gated, wout[:, mine_cols], preferred_element_type=F32).astype(BF16)
 
     idx = chosen[...]
     wts = weights[...]
@@ -152,24 +166,13 @@
         extra = jnp.where(lane == i, slot, extra)
         extra = jnp.where(lane == TOPK + i, w_hi, extra)
         extra = jnp.where(lane == 2 * TOPK + i, w - w_hi, extra)
-    tokens[0, :, half:] = extra.astype(BF16)
-
-    def remote(src, dst, send, recv, peer):
-        return pltpu.make_async_remote_copy(
-            src_ref=src, dst_ref=dst, send_sem=send, recv_sem=recv, device_id=peer, device_id_type=MESH
-        )
-
-    get_wout.wait()
-    tp_tx[...] = jnp.dot(gated, wout[:, other_cols], preferred_element_type=F32).astype(BF16)
-    pl.semaphore_wait(barrier, len(peers))
-    swap = remote(tp_tx, tp_rx, tp_s, tp_r, partner)
-    swap.start()
-    own_mix = jnp.dot(gated, wout[:, mine_cols], preferred_element_type=F32).astype(BF16)
+    tokens[z, :, half:] = extra.astype(BF16)
+
     base = hidden[...].astype(F32)
     swap.wait()
     mixed = own_mix.astype(F32) + tp_rx[...].astype(F32)
     resid = (base + mixed).astype(BF16)
-    tokens[0, :, :half] = resid
+    tokens[z, :, :half] = resid
 
     def update_states():
         u_hi = u.astype(BF16).astype(F32)
@@ -184,139 +187,211 @@
                     h = g * per_group + j
                     new_state[s, h] = decay[s : s + 1, h : h + 1] * state[s, h] + outer[j * width : (j + 1) * width]
 
-    copies, arrived = [], {}
-    for origin, hops in FIRST + FAN:
-        if origin == FAN[0][0]:
-            update_states()
-        if origin:
-            arrived.pop(origin).wait_recv()
-        for hop in hops:
-            q = len(copies)
-            lands = (origin + hop) % nz
-            copies.append(remote(tokens.at[origin], tokens.at[lands], z_s.at[q], z_r.at[q], along_z(hop)))
-            arrived[lands] = copies[q]
-            copies[q].start()
-    for copy in arrived.values():
-        copy.wait_recv()
-
-    held = tokens[...].astype(F32).reshape(nz * seqs, half + LANES)
-    info = held[:, half:]
-    info = info + jnp.where(iota(info.shape, 1) < TOPK, 0.0, pltpu.roll(info, LANES - TOPK, 1))
-    row_z = iota((nz * seqs, rows), 0) // seqs
-    col = iota((nz * seqs, rows), 1)
-    slot_of = ((z * X_SIDE + col // slots) * CAP + col % CAP).astype(F32)
-    same_z = (col % slots) // CAP == row_z
-    takes = jnp.zeros((nz * seqs, rows), F32)
-    mixing = jnp.zeros((nz * seqs, rows), F32)
-    for i in range(TOPK):
-        hit = same_z & (info[:, i : i + 1] == slot_of)
-        takes = jnp.where(hit, 1.0, takes)
-        mixing = jnp.where(hit, info[:, TOPK + i : TOPK + i + 1], mixing)
-    mix_hi = mixing.astype(BF16)
-    mix_lo = (mixing - mix_hi.astype(F32)).astype(BF16)
-    picked = jnp.dot(takes.T.astype(BF16), held[:, :half].astype(BF16), preferred_element_type=F32).astype(BF16)
-    pick_tx[...] = picked.reshape(X_SIDE, slots, half)
-
-    def at_x(ref, d):
-        return ref.at[(x + d + X_SIDE) % X_SIDE]
-
-    order = [2, 1, 3]
-    sent = []
-    for i, d in enumerate(order):
-        sent.append(remote(at_x(pick_tx, d), pick_rx.at[x], x_s.at[i], x_r.at[i], along_x(d)))
-        sent[i].start()
-    pick_rx[x] = pick_tx[x]
-    shared = [remote(pick_tx.at[x], pick_other.at[x], o_s.at[3], o_r.at[3], partner)]
-    shared[0].start()
-    for i in (1, 2, 0):
-        d = order[i]
-        got = at_x(pick_rx, -d)
-        remote(got, got, x_s.at[i], x_r.at[i], along_x(d)).wait_recv()
-        shared.append(remote(got, at_x(pick_other, -d), o_s.at[i], o_r.at[i], partner))
-        shared[-1].start()
+    def origin_of(back):
+        return (z + nz - back) % nz
+
+    def token_copy(back, hop):
+        block = tokens.at[origin_of(back)]
+        lands = (back + hop) % nz
+        return remote(block, block, z_s.at[lands], z_r.at[lands], along_z(hop))
+
+    def token_arrives(back):
+        block = tokens.at[origin_of(back)]
+        remote(block, block, z_s.at[back], z_r.at[back], partner).wait_recv()
+
+    def relay(back):
+        token_arrives(back)
+        for hop in FAN[back]:
+            token_copy(back, hop).start()
+
+    def earlier_first(step):
+        up_first = origin_of(RELAYS[0]) < origin_of(RELAYS[1])
+
+        @pl.when(up_first)
+        def _():
+            step(RELAYS[0])
+            step(RELAYS[1])
+
+        @pl.when(jnp.logical_not(up_first))
+        def _():
+            step(RELAYS[1])
+            step(RELAYS[0])
+
+    for hop in FIRST:
+        token_copy(0, hop).start()
+    update_states()
+    earlier_first(relay)
+
+    def at_x(ref, part, d):
+        return ref.at[part, (x + d + X_SIDE) % X_SIDE]
+
+    def across(part):
+        for origin in range(part * some, (part + 1) * some):
+            back = (z + nz - origin) % nz
+            awaited = back != 0
+            for done in RELAYS:
+                awaited = awaited & (back != done)
+
+            @pl.when(awaited)
+            def _(back=back):
+                token_arrives(back)
+
+        held = tokens[part * some : (part + 1) * some].astype(F32).reshape(some * seqs, half + LANES)
+        info = held[:, half:]
+        info = info + jnp.where(iota(info.shape, 1) < TOPK, 0.0, pltpu.roll(info, LANES - TOPK, 1))
+        shape = (some * seqs, X_SIDE * slots)
+        col = iota(shape, 1)
+        slot_of = ((z * X_SIDE + col // slots) * CAP + col % CAP).astype(F32)
+        same_z = (col % slots) // CAP == iota(shape, 0) // seqs
+        takes = jnp.zeros(shape, F32)
+        mixing = jnp.zeros(shape, F32)
+        for i in range(TOPK):
+            hit = same_z & (info[:, i : i + 1] == slot_of)
+            takes = jnp.where(hit, 1.0, takes)
+            mixing = jnp.where(hit, info[:, TOPK + i : TOPK + i + 1], mixing)
+        mix_hi = mixing.astype(BF16)
+        mix_lo = (mixing - mix_hi.astype(F32)).astype(BF16)
+        picked = jnp.dot(takes.T.astype(BF16), held[:, :half].astype(BF16), preferred_element_type=F32).astype(BF16)
+        pick_tx[part] = picked.reshape(X_SIDE, slots, half)
+        sent = []
+        for i, d in enumerate(ORDER):
+            sent.append(remote(at_x(pick_tx, part, d), pick_rx.at[part, x], x_s.at[part, i], x_r.at[part, i], along_x(d)))
+            sent[i].start()
+        pick_rx[part, x] = pick_tx[part, x]
+        shared = [remote(pick_tx.at[part, x], pick_other.at[part, x], o_s.at[part, 3], o_r.at[part, 3], partner)]
+        shared[0].start()
+        return sent, shared, (mix_hi, mix_lo)
+
+    def share(part, shared):
+        for i in (1, 2, 0):
+            d = ORDER[i]
+            got = at_x(pick_rx, part, -d)
+            remote(got, got, x_s.at[part, i], x_r.at[part, i], along_x(d)).wait_recv()
+            shared.append(remote(got, at_x(pick_other, part, -d), o_s.at[part, i], o_r.at[part, i], partner))
+            shared[-1].start()
 
     def project(values, cols):
-        f = values[...].reshape(rows, half).astype(F32)
+        f = values.reshape(rows, half).astype(F32)
         scaled = (f * norm[cols].astype(F32)[None, :]).astype(BF16)
         dims = (((1,), (1,)), ((), ()))
         g = lax.dot_general(scaled, wg[:, cols], dims, preferred_element_type=F32)
         u = lax.dot_general(scaled, wu[:, cols], dims, preferred_element_type=F32)
         return g, u, jnp.sum(f * f, axis=1, keepdims=True)
 
+    def activate(part, shared):
+        g0, u0, s0 = project(pick_rx[part], mine_cols)
+        for copy in shared:
+            copy.wait_recv()
+        g1, u1, s1 = project(pick_other[part], other_cols)
+        inv = lax.rsqrt((s0 + s1) / (2 * half) + EPSILON)
+        return (silu(inv * (g0 + g1)) * (inv * (u0 + u1))).astype(BF16)
+
+    def down(part, act):
+        down_tx[part] = jnp.dot(act, wd[:, other_cols], preferred_element_type=F32).astype(BF16)
+        trade = remote(down_tx.at[part], down_rx.at[part], d_s.at[part], d_r.at[part], partner)
+        trade.start()
+        return trade, jnp.dot(act, wd[:, mine_cols], preferred_element_type=F32).astype(BF16)
+
+    def give_back(part, trade, own_down):
+        trade.wait_recv()
+        result = (own_down.astype(F32) + down_rx[part].astype(F32)).astype(BF16)
+        back_tx[part] = result.reshape(X_SIDE, slots, half)
+        returned = []
+        for i, d in enumerate(ORDER):
+            returned.append(remote(at_x(back_tx, part, d), back_rx.at[part, x], b_s.at[part, i], b_r.at[part, i], along_x(d)))
+            returned[i].start()
+        back_rx[part, x] = back_tx[part, x]
+        return returned
+
+    def collect(part, mix):
+        for i, d in enumerate(ORDER):
+            got = at_x(back_rx, part, -d)
+            remote(got, got, b_s.at[part, i], b_r.at[part, i], along_x(d)).wait_recv()
+        rows_back = back_rx[part].reshape(rows, half)
+        total = jnp.dot(mix[0], rows_back, preferred_element_type=F32) + jnp.dot(mix[1], rows_back, preferred_element_type=F32)
+        total = total.reshape(some, seqs, half)
+        sums[part * some : (part + 1) * some] = total
+        sums_bf[part * some : (part + 1) * some] = total.astype(BF16)
+
+    near = [hop for hop in FIRST if hop % nz not in RELAYS]
+    routes = {}
+    for i, hop in enumerate(near):
+        routes[hop % nz] = (-hop, last_rx.at[i])
+    for back in RELAYS:
+        for hop in FAN[back]:
+            routes[(back + hop) % nz] = (-hop, relay_rx.at[len(routes) - len(near)])
+    leaves = {back: [routes[(back + hop) % nz][1] for hop in FAN[back]] for back in RELAYS}
+
+    def sum_copy(back):
+        hop, lands = routes[back]
+        return remote(sums_bf.at[origin_of(back)], lands, h_s.at[back], h_r.at[back], along_z(hop))
+
+    def send_sums(part):
+        for back in routes:
+
+            @pl.when(origin_of(back) // some == part)
+            def _(back=back):
+                sum_copy(back).start()
+
+    def relay_copy(back):
+        i = RELAYS.index(back)
+        hop = FIRST[i]
+        return remote(relay_tx.at[i], last_rx.at[len(near) + i], h_s.at[back], h_r.at[back], along_z(-hop))
+
+    def relay_sum(back):
+        total = sums[origin_of(back)]
+        for hop, landed in zip(FAN[back], leaves[back]):
+            sum_copy((back + hop) % nz).wait_recv()
+            total = total + landed[...].astype(F32)
+        relay_tx[RELAYS.index(back)] = total.astype(BF16)
+        relay_copy(back).start()
+
+    sent_e, shared_e, mix_e = across(0)
+    sent_l, shared_l, mix_l = across(1)
+    share(0, shared_e)
     for load in loads:
         load.wait()
-    g0, u0, s0 = project(pick_rx, mine_cols)
-    for copy in shared:
-        copy.wait_recv()
-    g1, u1, s1 = project(pick_other, other_cols)
-    inv = lax.rsqrt((s0 + s1) / (2 * half) + EPSILON)
-    act = (silu(inv * (g0 + g1)) * (inv * (u0 + u1))).astype(BF16)
-    down_tx[...] = jnp.dot(act, wd[:, other_cols], preferred_element_type=F32).astype(BF16)
-    trade = remote(down_tx, down_rx, d_s, d_r, partner)
-    trade.start()
-    own_down = jnp.dot(act, wd[:, mine_cols], preferred_element_type=F32).astype(BF16)
-    trade.wait_recv()
-    result = (own_down.astype(F32) + down_rx[...].astype(F32)).astype(BF16)
-    back_tx[...] = result.reshape(X_SIDE, slots, half)
-
-    returned = []
-    for i, d in enumerate(order):
-        returned.append(remote(at_x(back_tx, d), back_rx.at[x], b_s.at[i], b_r.at[i], along_x(d)))
-        returned[i].start()
-    back_rx[x] = back_tx[x]
-    for i, d in enumerate(order):
-        got = at_x(back_rx, -d)
-        remote(got, got, b_s.at[i], b_r.at[i], along_x(d)).wait_recv()
-    rows_back = back_rx[...].reshape(rows, half)
-    part = jnp.dot(mix_hi, rows_back, preferred_element_type=F32) + jnp.dot(mix_lo, rows_back, preferred_element_type=F32)
-    part = part.reshape(nz, seqs, half)
-    sums[...] = part
-    sums_bf[...] = part.astype(BF16)
-
-    parts = []
-
-    def send(src, dst, hop):
-        q = len(parts)
-        parts.append(remote(src, dst, h_s.at[q], h_r.at[q], along_z(hop)))
-        parts[q].start()
-        return parts[q]
-
-    gathered = {}
-    n = 0
-    for origin, hops in FAN:
-        for hop in hops:
-            gathered.setdefault(origin, []).append((send(sums_bf.at[(origin + hop) % nz], relay_rx.at[n], -hop), n))
-            n += 1
-    finals = []
-    (_, first_hops), = FIRST
-    for hop in first_hops[len(FAN):]:
-        finals.append(send(sums_bf.at[hop % nz], last_rx.at[len(finals)], -hop))
-    for i, (origin, _) in enumerate(FAN):
-        total = sums[origin]
-        for copy, at in gathered[origin]:
-            copy.wait_recv()
-            total = total + relay_rx[at].astype(F32)
-        relay_tx[i] = total.astype(BF16)
-        finals.append(send(relay_tx.at[i], last_rx.at[len(finals)], -first_hops[i]))
-    total = resid.astype(F32) + sums[0]
-    for i, copy in enumerate(finals):
-        copy.wait_recv()
+    act_e = activate(0, shared_e)
+    trade_e, own_e = down(0, act_e)
+    share(1, shared_l)
+    act_l = activate(1, shared_l)
+    trade_l, own_l = down(1, act_l)
+    returned_e = give_back(0, trade_e, own_e)
+    returned_l = give_back(1, trade_l, own_l)
+    collect(0, mix_e)
+    send_sums(0)
+    collect(1, mix_l)
+    send_sums(1)
+    earlier_first(relay_sum)
+    total = resid.astype(F32) + sums[z]
+    for i, hop in enumerate(near):
+        sum_copy(hop % nz).wait_recv()
         total = total + last_rx[i].astype(F32)
+    for i, back in enumerate(RELAYS):
+        relay_copy(back).wait_recv()
+        total = total + last_rx[len(near) + i].astype(F32)
     out[...] = total.astype(BF16)
 
-    swap_done = [*copies, *sent, *shared, trade, *returned, *parts]
-    for copy in swap_done:
+    for copy in [*sent_e, *sent_l, *shared_e, *shared_l, trade_e, trade_l, *returned_e, *returned_l]:
         copy.wait_send()
+    for hop in FIRST:
+        token_copy(0, hop).wait_send()
+    for back in RELAYS:
+        for hop in FAN[back]:
+            token_copy(back, hop).wait_send()
+        relay_copy(back).wait_send()
+    for back in routes:
+        sum_copy(back).wait_send()
 
 
 def layer(ep, *args):
     hidden, head_in, gate, b_map, c_map, raw_step, hist, taps, state, rate, extra, skip, wout, norm, chosen, weights, wg, wu, wd = args
     seqs, half = hidden.shape
     nz = ep // X_SIDE
-    slots = nz * CAP
+    slots = nz // 2 * CAP
     rows = X_SIDE * slots
-    far = sum(len(hops) for _, hops in FAN)
-    near = len(FIRST[0][1])
+    far = sum(len(hops) for hops in FAN.values())
+    near = len(FIRST)
     vmem = pl.BlockSpec(memory_space=pltpu.VMEM)
     hbm = pl.BlockSpec(memory_space=pltpu.HBM)
     dma = pltpu.SemaphoreType.DMA
@@ -341,16 +416,16 @@
             room(hidden),
             room(hidden),
             pltpu.VMEM((nz, seqs, half + LANES), BF16),
-            *(pltpu.VMEM((X_SIDE, slots, half), BF16) for _ in range(3)),
-            *(pltpu.VMEM((rows, half), BF16) for _ in range(2)),
-            *(pltpu.VMEM((X_SIDE, slots, half), BF16) for _ in range(2)),
+            *(pltpu.VMEM((2, X_SIDE, slots, half), BF16) for _ in range(3)),
+            *(pltpu.VMEM((2, rows, half), BF16) for _ in range(2)),
+            *(pltpu.VMEM((2, X_SIDE, slots, half), BF16) for _ in range(2)),
             pltpu.VMEM((nz, seqs, half), F32),
             pltpu.VMEM((nz, seqs, half), BF16),
             pltpu.VMEM((far, seqs, half), BF16),
             pltpu.VMEM((2, seqs, half), BF16),
             pltpu.VMEM((near, seqs, half), BF16),
-            dma((14 + seqs,)), dma((4,)), one, one, dma((nz - 1,)), dma((nz - 1,)), dma((3,)), dma((3,)), dma((4,)), dma((4,)),
-            one, one, dma((3,)), dma((3,)), dma((nz - 1,)), dma((nz - 1,)),
+            dma((14 + seqs,)), dma((4,)), one, one, dma((nz,)), dma((nz,)), dma((2, 3)), dma((2, 3)), dma((2, 4)), dma((2, 4)),
+            dma((2,)), dma((2,)), dma((2, 3)), dma((2, 3)), dma((nz,)), dma((nz,)),
         ],
         compiler_params=pltpu.CompilerParams(collective_id=0, has_side_effects=True, vmem_limit_bytes=VMEM_BYTES),
     )(*(pltpu.with_memory_space_constraint(a, pltpu.HBM) for a in args))

time: 66.2 us -> 67.2 us (1.015)
  Pallas kernels: 65.4 us -> 66.3 us
    pallas_call x1, Pallas kernels: 63.3 us -> 64.3 us  [layer(): pl.pallas_call(layer_kernel, name='layer', in_specs=[hbm] * len(args), ou...]
where the time goes in v3:
time: 67.2 us; the launch traced here: 67 us
  Pallas kernels  66.3 us (99%)
    pallas_call x1, Pallas kernels, layer(): pl.pallas_call(layer_kernel, name='layer', in_specs=[hbm] * len(args), ou...  64.3 us
    pallas_call x1, Pallas kernels, store(): pl.pallas_call(store_kernel, name='store', in_specs=[pl.BlockSpec(memory_...  2.05 us

profile of v3, /device:TPU:40, one launch (start us, length us, event | category | flops | bytes accessed | tf_op | source)
XLA Modules:
  0.0 67.0 jit_solution(17084705968450868146)
XLA Ops:
  0.6 64.3 %layer.1 = (bf16[8,1024]{1,0:T(8,128)(2,1)S(1)}, f32[8,16,64,64]{3,2,1,0:T(8,128)S(1)}, bf16[3,8,1024]{2,1,0:T(8,128)(2,1)S(1)}) custom-call(bf16[8,1024]{1,0:T(8,128)(2,1)} %hidden_h.1, bf16[8,1024]{1,0:T(8,128)(2,1)} %head_in_h.1, bf16[8,1024]{1,0:T(8,128)(2,1)} %gate_h.1, bf16[8,128]{1,0:T(8,128)(2,1)} %b_map_h.1, bf16[8,128]{1,0:T(8,128)(2,1)} %c_map_h.1, ...), custom_call_target="tpu_custom_call" | custom-call | tf_op jit(solution)/shard_map/layer/pallas_call | solution.py:403
  64.9 2.0 %store.1 = (bf16[8,1024]{1,0:T(8,128)(2,1)}, f32[8,16,64,64]{3,2,1,0:T(8,128)}, bf16[3,8,1024]{2,1,0:T(8,128)(2,1)}) custom-call(bf16[8,1024]{1,0:T(8,128)(2,1)S(1)} %get-tuple-element.9.refs_0_, f32[8,16,64,64]{3,2,1,0:T(8,128)S(1)} %get-tuple-element.10.refs_1_, bf16[3,8,1024]{2,1,0:T(8,128)(2,1)S(1)} %get-tuple-element.11.refs_2_), custom_call_target="tpu_custom_call" | custom-call | tf_op jit(solution)/shard_map/store/pallas_call | solution.py:445

commit v4 on v3

--- a/solution.py
+++ b/solution.py
@@ -16,9 +16,10 @@
 CAP = 2
 EPSILON = 1e-06
 X_SIDE = 4
-FIRST = (5, -5, 2, -2, 1, -1)
-RELAYS = (5, 11)
-FAN = {5: (3, 2, -2, 1, -1), 11: (-2, 2, -1, 1)}
+FIRST = [(0, (4, -4, 3, -3, 2, -2, 1, -1))]
+FAN = [(4, (4, 3, 2, 1)), (12, (-3, -2, -1))]
+BLOCKS = (0, 1, 15, 2, 14, 4, 12, 3, 13, 5, 6, 7, 8, 9, 10, 11)
+PLACE = {block: place for place, block in enumerate(BLOCKS)}
 ORDER = (2, 1, 3)
 LANES = 128
 HIGH = lax.Precision.HIGHEST
@@ -40,8 +41,8 @@
 def layer_kernel(
     hidden_h, head_in_h, gate_h, b_map_h, c_map_h, raw_step_h, hist_h, taps_h, state_h, rate_h, extra_h, skip_h, wout_h,
     norm_h, chosen_h, weights_h, wg_h, wu_h, wd_h,
-    out, new_state, new_hist,
-    hidden, head_in, gate, b_map, c_map, raw_step, hist, taps, state, rate, extra_decay, skip, wout,
+    out_h, new_state_h, new_hist_h,
+    out, new_state, new_hist, hidden, head_in, gate, b_map, c_map, raw_step, hist, taps, state, rate, extra_decay, skip, wout,
     norm, chosen, weights, wg, wu, wd,
     tp_tx, tp_rx, tokens, pick_tx, pick_rx, pick_other, down_tx, down_rx, back_tx, back_rx,
     sums, sums_bf, relay_rx, relay_tx, last_rx,
@@ -66,32 +67,42 @@
     mine_cols = pl.ds(pl.multiple_of(core * half, half), half)
     other_cols = pl.ds(pl.multiple_of(other * half, half), half)
 
+    pairs = [(c_map_h, c_map), (head_in_h, head_in), (hist_h, hist), (taps_h, taps), (raw_step_h, raw_step), (extra_h, extra_decay),
+             (rate_h, rate), (skip_h, skip), (b_map_h, b_map), (gate_h, gate), (hidden_h, hidden), (chosen_h, chosen),
+             (weights_h, weights), (norm_h, norm)]
+    small = [pltpu.make_async_copy(src, dst, in_sem.at[i]) for i, (src, dst) in enumerate(pairs)]
+    two = seqs // 4
+    fetch = [pltpu.make_async_copy(state_h.at[pl.ds(i * two, two)], state.at[pl.ds(i * two, two)], in_sem.at[len(pairs) + i]) for i in range(4)]
+    get_wout = pltpu.make_async_copy(wout_h, wout, w_sem.at[0])
+    loads = [pltpu.make_async_copy(src, dst, w_sem.at[1 + i])
+             for i, (src, dst) in enumerate([(wg_h.at[0], wg), (wu_h.at[0], wu), (wd_h.at[0], wd)])]
+    for copy in [small[0], *fetch, *small[1:], get_wout]:
+        copy.start()
     barrier = pltpu.get_barrier_semaphore()
-    steps = sorted({s * h for hops in (FIRST, *FAN.values()) for h in hops for s in (1, -1)})
+    steps = sorted({s * h for _, hops in FIRST + FAN for h in hops for s in (1, -1)})
     peers = [along_z(h) for h in steps] + [along_x(d) for d in range(1, X_SIDE)] + [partner]
     for peer in peers:
         pl.semaphore_signal(barrier, inc=1, device_id=peer, device_id_type=MESH)
-    pairs = [(head_in_h, head_in), (hist_h, hist), (taps_h, taps), (raw_step_h, raw_step), (extra_h, extra_decay), (rate_h, rate),
-             (skip_h, skip), (b_map_h, b_map), (c_map_h, c_map), (gate_h, gate), (hidden_h, hidden), (chosen_h, chosen),
-             (weights_h, weights), (norm_h, norm)]
-    small = [pltpu.make_async_copy(src, dst, in_sem.at[i]) for i, (src, dst) in enumerate(pairs)]
-    for copy in small:
-        copy.start()
-    fetch = [pltpu.make_async_copy(state_h.at[s], state.at[s], in_sem.at[len(pairs) + s]) for s in range(seqs)]
-    for copy in fetch:
-        copy.start()
-    get_wout = pltpu.make_async_copy(wout_h, wout, w_sem.at[0])
-    get_wout.start()
-    loads = [pltpu.make_async_copy(src, dst, w_sem.at[1 + i])
-             for i, (src, dst) in enumerate([(wg_h.at[0], wg), (wu_h.at[0], wu), (wd_h.at[0], wd)])]
-    for copy in small:
-        copy.wait()
 
     heads = raw_step.shape[1]
     width = half // heads
     groups = b_map.shape[1] // STATE_DIM
     per_group = heads // groups
     chans = per_group * width
+    small[0].wait()
+    c_all = c_map[...].astype(F32)
+    row_c = iota((seqs, STATE_DIM), 0)
+    seen = [jnp.zeros((seqs, chans), F32) for _ in range(groups)]
+    for s in range(seqs):
+        if s % two == 0:
+            fetch[s // two].wait()
+        for g in range(groups):
+            c_g = jnp.where(row_c == s, c_all[:, g * STATE_DIM : (g + 1) * STATE_DIM], 0.0).astype(BF16)
+            held = state[s, g * per_group : (g + 1) * per_group].reshape(chans, STATE_DIM).astype(BF16)
+            seen[g] = seen[g] + lax.dot_general(c_g, held, (((1,), (1,)), ((), ())), preferred_element_type=F32)
+    for copy in small[1:]:
+        copy.wait()
+
     fresh_in = head_in[...]
     for i in range(2):
         new_hist[i] = hist[i + 1]
@@ -117,20 +128,10 @@
         skips = jnp.where(col == h, skip[h], skips)
     opened = silu(gate[...].astype(F32))
     b_all = b_map[...].astype(F32)
-    c_all = c_map[...].astype(F32)
-
-    row_c = iota((seqs, STATE_DIM), 0)
     read = []
     for g in range(groups):
         cols = slice(g * STATE_DIM, (g + 1) * STATE_DIM)
         read.append(u[:, g * chans : (g + 1) * chans] * jnp.sum(b_all[:, cols] * c_all[:, cols], axis=1, keepdims=True))
-    seen = [jnp.zeros((seqs, chans), F32) for _ in range(groups)]
-    for s in range(seqs):
-        fetch[s].wait()
-        for g in range(groups):
-            c_g = jnp.where(row_c == s, c_all[:, g * STATE_DIM : (g + 1) * STATE_DIM], 0.0).astype(BF16)
-            held = state[s, g * per_group : (g + 1) * per_group].reshape(chans, STATE_DIM).astype(BF16)
-            seen[g] = seen[g] + lax.dot_general(c_g, held, (((1,), (1,)), ((), ())), preferred_element_type=F32)
     for load in loads:
         load.start()
     readout = decays * jnp.concatenate(seen, axis=1) + jnp.concatenate(read, axis=1) + skips * conv
@@ -166,13 +167,13 @@
         extra = jnp.where(lane == i, slot, extra)
         extra = jnp.where(lane == TOPK + i, w_hi, extra)
         extra = jnp.where(lane == 2 * TOPK + i, w - w_hi, extra)
-    tokens[z, :, half:] = extra.astype(BF16)
+    tokens[0, :, half:] = extra.astype(BF16)
 
     base = hidden[...].astype(F32)
     swap.wait()
     mixed = own_mix.astype(F32) + tp_rx[...].astype(F32)
     resid = (base + mixed).astype(BF16)
-    tokens[z, :, :half] = resid
+    tokens[0, :, :half] = resid
 
     def update_states():
         u_hi = u.astype(BF16).astype(F32)
@@ -187,55 +188,34 @@
                     h = g * per_group + j
                     new_state[s, h] = decay[s : s + 1, h : h + 1] * state[s, h] + outer[j * width : (j + 1) * width]
 
-    def origin_of(back):
-        return (z + nz - back) % nz
-
-    def token_copy(back, hop):
-        block = tokens.at[origin_of(back)]
-        lands = (back + hop) % nz
-        return remote(block, block, z_s.at[lands], z_r.at[lands], along_z(hop))
-
-    def token_arrives(back):
-        block = tokens.at[origin_of(back)]
-        remote(block, block, z_s.at[back], z_r.at[back], partner).wait_recv()
-
-    def relay(back):
-        token_arrives(back)
-        for hop in FAN[back]:
-            token_copy(back, hop).start()
-
-    def earlier_first(step):
-        up_first = origin_of(RELAYS[0]) < origin_of(RELAYS[1])
-
-        @pl.when(up_first)
-        def _():
-            step(RELAYS[0])
-            step(RELAYS[1])
-
-        @pl.when(jnp.logical_not(up_first))
-        def _():
-            step(RELAYS[1])
-            step(RELAYS[0])
-
-    for hop in FIRST:
-        token_copy(0, hop).start()
+    copies, arrived = [], {}
+
+    def spread_from(origin, hops):
+        for hop in hops:
+            q = len(copies)
+            lands = (origin + hop) % nz
+            copies.append(remote(tokens.at[PLACE[origin]], tokens.at[PLACE[lands]], z_s.at[q], z_r.at[q], along_z(hop)))
+            arrived[lands] = copies[q]
+            copies[q].start()
+
+    for origin, hops in FIRST:
+        spread_from(origin, hops)
     update_states()
-    earlier_first(relay)
+    keep = [pltpu.make_async_copy(new_state, new_state_h, w_sem.at[4]), pltpu.make_async_copy(new_hist, new_hist_h, w_sem.at[5]),
+            pltpu.make_async_copy(out, out_h, w_sem.at[6])]
+    for copy in keep[:2]:
+        copy.start()
+    for origin, hops in FAN:
+        arrived.pop(origin).wait_recv()
+        spread_from(origin, hops)
 
     def at_x(ref, part, d):
         return ref.at[part, (x + d + X_SIDE) % X_SIDE]
 
     def across(part):
-        for origin in range(part * some, (part + 1) * some):
-            back = (z + nz - origin) % nz
-            awaited = back != 0
-            for done in RELAYS:
-                awaited = awaited & (back != done)
-
-            @pl.when(awaited)
-            def _(back=back):
-                token_arrives(back)
-
+        for place in range(part * some, (part + 1) * some):
+            if BLOCKS[place] in arrived:
+                arrived.pop(BLOCKS[place]).wait_recv()
         held = tokens[part * some : (part + 1) * some].astype(F32).reshape(some * seqs, half + LANES)
         info = held[:, half:]
         info = info + jnp.where(iota(info.shape, 1) < TOPK, 0.0, pltpu.roll(info, LANES - TOPK, 1))
@@ -292,7 +272,7 @@
         trade.start()
         return trade, jnp.dot(act, wd[:, mine_cols], preferred_element_type=F32).astype(BF16)
 
-    def give_back(part, trade, own_down):
+    def back(part, trade, own_down):
         trade.wait_recv()
         result = (own_down.astype(F32) + down_rx[part].astype(F32)).astype(BF16)
         back_tx[part] = result.reshape(X_SIDE, slots, half)
@@ -313,75 +293,62 @@
         sums[part * some : (part + 1) * some] = total
         sums_bf[part * some : (part + 1) * some] = total.astype(BF16)
 
-    near = [hop for hop in FIRST if hop % nz not in RELAYS]
-    routes = {}
-    for i, hop in enumerate(near):
-        routes[hop % nz] = (-hop, last_rx.at[i])
-    for back in RELAYS:
-        for hop in FAN[back]:
-            routes[(back + hop) % nz] = (-hop, relay_rx.at[len(routes) - len(near)])
-    leaves = {back: [routes[(back + hop) % nz][1] for hop in FAN[back]] for back in RELAYS}
-
-    def sum_copy(back):
-        hop, lands = routes[back]
-        return remote(sums_bf.at[origin_of(back)], lands, h_s.at[back], h_r.at[back], along_z(hop))
-
-    def send_sums(part):
-        for back in routes:
-
-            @pl.when(origin_of(back) // some == part)
-            def _(back=back):
-                sum_copy(back).start()
-
-    def relay_copy(back):
-        i = RELAYS.index(back)
-        hop = FIRST[i]
-        return remote(relay_tx.at[i], last_rx.at[len(near) + i], h_s.at[back], h_r.at[back], along_z(-hop))
-
-    def relay_sum(back):
-        total = sums[origin_of(back)]
-        for hop, landed in zip(FAN[back], leaves[back]):
-            sum_copy((back + hop) % nz).wait_recv()
-            total = total + landed[...].astype(F32)
-        relay_tx[RELAYS.index(back)] = total.astype(BF16)
-        relay_copy(back).start()
-
-    sent_e, shared_e, mix_e = across(0)
-    sent_l, shared_l, mix_l = across(1)
-    share(0, shared_e)
+    sent_n, shared_n, mix_n = across(0)
+    sent_f, shared_f, mix_f = across(1)
+    share(0, shared_n)
     for load in loads:
         load.wait()
-    act_e = activate(0, shared_e)
-    trade_e, own_e = down(0, act_e)
-    share(1, shared_l)
-    act_l = activate(1, shared_l)
-    trade_l, own_l = down(1, act_l)
-    returned_e = give_back(0, trade_e, own_e)
-    returned_l = give_back(1, trade_l, own_l)
-    collect(0, mix_e)
-    send_sums(0)
-    collect(1, mix_l)
-    send_sums(1)
-    earlier_first(relay_sum)
-    total = resid.astype(F32) + sums[z]
-    for i, hop in enumerate(near):
-        sum_copy(hop % nz).wait_recv()
+    act_n = activate(0, shared_n)
+    share(1, shared_f)
+    act_f = activate(1, shared_f)
+    trade_f, own_f = down(1, act_f)
+    trade_n, own_n = down(0, act_n)
+    returned_f = back(1, trade_f, own_f)
+    returned_n = back(0, trade_n, own_n)
+
+    parts = []
+
+    def send(src, dst, hop):
+        q = len(parts)
+        parts.append(remote(src, dst, h_s.at[q], h_r.at[q], along_z(hop)))
+        parts[q].start()
+        return parts[q]
+
+    gathered = {origin: [] for origin, _ in FAN}
+
+    def send_far(part):
+        for origin, hops in FAN:
+            for hop in hops:
+                place = PLACE[(origin + hop) % nz]
+                if place // some == part:
+                    n = sum(len(g) for g in gathered.values())
+                    gathered[origin].append((send(sums_bf.at[place], relay_rx.at[n], -hop), n))
+
+    collect(1, mix_f)
+    send_far(1)
+    collect(0, mix_n)
+    send_far(0)
+    finals = []
+    (_, first_hops), = FIRST
+    for hop in first_hops[len(FAN):]:
+        finals.append(send(sums_bf.at[PLACE[hop % nz]], last_rx.at[len(finals)], -hop))
+    for i, (origin, _) in enumerate(FAN):
+        total = sums[PLACE[origin]]
+        for copy, at in gathered[origin]:
+            copy.wait_recv()
+            total = total + relay_rx[at].astype(F32)
+        relay_tx[i] = total.astype(BF16)
+        finals.append(send(relay_tx.at[i], last_rx.at[len(finals)], -first_hops[i]))
+    total = resid.astype(F32) + sums[0]
+    for i, copy in enumerate(finals):
+        copy.wait_recv()
         total = total + last_rx[i].astype(F32)
-    for i, back in enumerate(RELAYS):
-        relay_copy(back).wait_recv()
-        total = total + last_rx[len(near) + i].astype(F32)
     out[...] = total.astype(BF16)
-
-    for copy in [*sent_e, *sent_l, *shared_e, *shared_l, trade_e, trade_l, *returned_e, *returned_l]:
+    keep[2].start()
+    for copy in [*copies, *sent_n, *sent_f, *shared_n, *shared_f, trade_n, trade_f, *returned_n, *returned_f, *parts]:
         copy.wait_send()
-    for hop in FIRST:
-        token_copy(0, hop).wait_send()
-    for back in RELAYS:
-        for hop in FAN[back]:
-            token_copy(back, hop).wait_send()
-        relay_copy(back).wait_send()
-    for back in routes:
-        sum_copy(back).wait_send()
+    for copy in keep:
+        copy.wait()
 
 
 def layer(ep, *args):
@@ -390,8 +357,8 @@
     nz = ep // X_SIDE
     slots = nz // 2 * CAP
     rows = X_SIDE * slots
-    far = sum(len(hops) for hops in FAN.values())
-    near = len(FIRST)
+    far = sum(len(hops) for _, hops in FAN)
+    near = len(FIRST[0][1])
     vmem = pl.BlockSpec(memory_space=pltpu.VMEM)
     hbm = pl.BlockSpec(memory_space=pltpu.HBM)
     dma = pltpu.SemaphoreType.DMA
@@ -404,13 +371,16 @@
         layer_kernel,
         name="layer",
         in_specs=[hbm] * len(args),
-        out_specs=[vmem, vmem, vmem],
+        out_specs=[pl.BlockSpec(memory_space=pl.ANY)] * 3,
         out_shape=[
             pltpu.VMEM(hidden.shape, BF16),
             pltpu.VMEM(state.shape, F32),
             pltpu.VMEM(hist.shape, BF16),
         ],
         scratch_shapes=[
+            room(hidden),
+            room(state),
+            room(hist),
             *(pltpu.SMEM(a.shape, F32) if a is rate or a is skip else room(a) for a in args[:16]),
             *(pltpu.VMEM(a.shape[1:], BF16) for a in (wg, wu, wd)),
             room(hidden),
@@ -424,8 +394,8 @@
             pltpu.VMEM((far, seqs, half), BF16),
             pltpu.VMEM((2, seqs, half), BF16),
             pltpu.VMEM((near, seqs, half), BF16),
-            dma((14 + seqs,)), dma((4,)), one, one, dma((nz,)), dma((nz,)), dma((2, 3)), dma((2, 3)), dma((2, 4)), dma((2, 4)),
-            dma((2,)), dma((2,)), dma((2, 3)), dma((2, 3)), dma((nz,)), dma((nz,)),
+            dma((14 + seqs,)), dma((7,)), one, one, dma((nz - 1,)), dma((nz - 1,)), dma((2, 3)), dma((2, 3)), dma((2, 4)), dma((2, 4)),
+            dma((2,)), dma((2,)), dma((2, 3)), dma((2, 3)), dma((nz - 1,)), dma((nz - 1,)),
         ],
         compiler_params=pltpu.CompilerParams(collective_id=0, has_side_effects=True, vmem_limit_bytes=VMEM_BYTES),
     )(*(pltpu.with_memory_space_constraint(a, pltpu.HBM) for a in args))
@@ -434,9 +404,13 @@
 def store_kernel(*refs):
     count = (len(refs) - 1) // 2
     sem = refs[-1]
-    copies = [pltpu.make_async_copy(refs[i], refs[count + i], sem.at[i]) for i in range(count)]
-    for copy in copies:
-        copy.start()
+    copies = []
+    for src, dst in zip(refs[:count], refs[count:-1]):
+        pieces = src.shape[0] if src.ndim == 4 else 1
+        for i in range(pieces):
+            piece = pl.ds(i * (src.shape[0] // pieces), src.shape[0] // pieces)
+            copies.append(pltpu.make_async_copy(src.at[piece], dst.at[piece], sem.at[len(copies)]))
+            copies[-1].start()
     for copy in copies:
         copy.wait()
 
@@ -445,10 +419,10 @@
     return pl.pallas_call(
         store_kernel,
         name="store",
-        in_specs=[pl.BlockSpec(memory_space=pltpu.VMEM)] * len(values),
+        in_specs=[pl.BlockSpec(memory_space=pl.ANY)] * len(values),
         out_specs=[pl.BlockSpec(memory_space=pltpu.HBM)] * len(values),
         out_shape=[pltpu.HBM(v.shape, v.dtype) for v in values],
-        scratch_shapes=[pltpu.SemaphoreType.DMA((len(values),))],
+        scratch_shapes=[pltpu.SemaphoreType.DMA((sum(v.shape[0] for v in values),))],
         compiler_params=pltpu.CompilerParams(vmem_limit_bytes=VMEM_BYTES),
     )(*(pltpu.with_memory_space_constraint(v, pltpu.VMEM) for v in values))
 

time: 67.2 us -> 64.4 us (0.958)
  Pallas kernels: 66.3 us -> 63.6 us
    pallas_call x1, Pallas kernels: 64.3 us -> 61.4 us  [layer(): pl.pallas_call(layer_kernel, name='layer', in_specs=[hbm] * len(args), ou...]
where the time goes in v4:
time: 64.4 us; the launch traced here: 64.3 us
  Pallas kernels  63.6 us (99%)
  between operations  0.65 us (1%)
    pallas_call x1, Pallas kernels, layer(): pl.pallas_call(layer_kernel, name='layer', in_specs=[hbm] * len(args), ou...  61.4 us
    pallas_call x1, Pallas kernels, store(): pl.pallas_call(store_kernel, name='store', in_specs=[pl.BlockSpec(memory_...  2.18 us

profile of v4, /device:TPU:40, one launch (start us, length us, event | category | flops | bytes accessed | tf_op | source)
XLA Modules:
  0.0 64.3 jit_solution(5018700708673545933)
XLA Ops:
  0.6 61.4 %layer.1 = (bf16[8,1024]{1,0:T(8,128)(2,1)S(1)}, f32[8,16,64,64]{3,2,1,0:T(8,128)S(1)}, bf16[3,8,1024]{2,1,0:T(8,128)(2,1)S(1)}) custom-call(bf16[8,1024]{1,0:T(8,128)(2,1)} %hidden_h.1, bf16[8,1024]{1,0:T(8,128)(2,1)} %head_in_h.1, bf16[8,1024]{1,0:T(8,128)(2,1)} %gate_h.1, bf16[8,128]{1,0:T(8,128)(2,1)} %b_map_h.1, bf16[8,128]{1,0:T(8,128)(2,1)} %c_map_h.1, ...), custom_call_target="tpu_custom_call" | custom-call | tf_op jit(solution)/shard_map/layer/pallas_call | solution.py:370
  62.1 2.2 %store.1 = (bf16[8,1024]{1,0:T(8,128)(2,1)}, f32[8,16,64,64]{3,2,1,0:T(8,128)}, bf16[3,8,1024]{2,1,0:T(8,128)(2,1)}) custom-call(bf16[8,1024]{1,0:T(8,128)(2,1)S(1)} %get-tuple-element.9.refs_0_, f32[8,16,64,64]{3,2,1,0:T(8,128)S(1)} %get-tuple-element.10.refs_1_, bf16[3,8,1024]{2,1,0:T(8,128)(2,1)S(1)} %get-tuple-element.11.refs_2_), custom_call_target="tpu_custom_call" | custom-call | tf_op jit(solution)/shard_map/store/pallas_call | solution.py:419

commit v5 on v4

--- a/solution.py
+++ b/solution.py
@@ -56,9 +56,14 @@
     me, core = lax.axis_index("ep"), lax.axis_index("tp")
     z, x = me // X_SIDE, me % X_SIDE
     other = 1 - core
+    turn = 1 - 2 * core
+
+    def spot(block):
+        here, there = PLACE[block], PLACE[(nz - block) % nz]
+        return here if here == there else jnp.where(core == 0, here, there)
 
     def along_z(d):
-        return {"ep": ((z + d + nz) % nz) * X_SIDE + x}
+        return {"ep": ((z + turn * d + nz) % nz) * X_SIDE + x}
 
     def along_x(d):
         return {"ep": z * X_SIDE + (x + d) % X_SIDE}
@@ -194,7 +199,7 @@
         for hop in hops:
             q = len(copies)
             lands = (origin + hop) % nz
-            copies.append(remote(tokens.at[PLACE[origin]], tokens.at[PLACE[lands]], z_s.at[q], z_r.at[q], along_z(hop)))
+            copies.append(remote(tokens.at[spot(origin)], tokens.at[spot(lands)], z_s.at[q], z_r.at[q], along_z(hop)))
             arrived[lands] = copies[q]
             copies[q].start()
 
@@ -213,9 +218,8 @@
         return ref.at[part, (x + d + X_SIDE) % X_SIDE]
 
     def across(part):
-        for place in range(part * some, (part + 1) * some):
-            if BLOCKS[place] in arrived:
-                arrived.pop(BLOCKS[place]).wait_recv()
+        for block in [b for b in arrived if part or {b, nz - b} & set(BLOCKS[:some])]:
+            arrived.pop(block).wait_recv()
         held = tokens[part * some : (part + 1) * some].astype(F32).reshape(some * seqs, half + LANES)
         info = held[:, half:]
         info = info + jnp.where(iota(info.shape, 1) < TOPK, 0.0, pltpu.roll(info, LANES - TOPK, 1))
@@ -319,10 +323,10 @@
     def send_far(part):
         for origin, hops in FAN:
             for hop in hops:
-                place = PLACE[(origin + hop) % nz]
-                if place // some == part:
+                block = (origin + hop) % nz
+                if PLACE[block] // some == part:
                     n = sum(len(g) for g in gathered.values())
-                    gathered[origin].append((send(sums_bf.at[place], relay_rx.at[n], -hop), n))
+                    gathered[origin].append((send(sums_bf.at[spot(block)], relay_rx.at[n], -hop), n))
 
     collect(1, mix_f)
     send_far(1)
@@ -330,15 +334,15 @@
     send_far(0)
     finals = []
     (_, first_hops), = FIRST
-    for hop in first_hops[len(FAN):]:
-        finals.append(send(sums_bf.at[PLACE[hop % nz]], last_rx.at[len(finals)], -hop))
     for i, (origin, _) in enumerate(FAN):
-        total = sums[PLACE[origin]]
+        total = sums[spot(origin)]
         for copy, at in gathered[origin]:
             copy.wait_recv()
             total = total + relay_rx[at].astype(F32)
         relay_tx[i] = total.astype(BF16)
         finals.append(send(relay_tx.at[i], last_rx.at[len(finals)], -first_hops[i]))
+    for hop in first_hops[len(FAN):]:
+        finals.append(send(sums_bf.at[spot(hop % nz)], last_rx.at[len(finals)], -hop))
     total = resid.astype(F32) + sums[0]
     for i, copy in enumerate(finals):
         copy.wait_recv()

time: 64.4 us -> 63.3 us (0.983)
  Pallas kernels: 63.6 us -> 62.6 us
    pallas_call x1, Pallas kernels: 61.4 us -> 60.4 us  [layer(): pl.pallas_call(layer_kernel, name='layer', in_specs=[hbm] * len(args), ou...]
where the time goes in v5:
time: 63.3 us; the launch traced here: 63.2 us
  Pallas kernels  62.6 us (99%)
  between operations  0.65 us (1%)
    pallas_call x1, Pallas kernels, layer(): pl.pallas_call(layer_kernel, name='layer', in_specs=[hbm] * len(args), ou...  60.4 us
    pallas_call x1, Pallas kernels, store(): pl.pallas_call(store_kernel, name='store', in_specs=[pl.BlockSpec(memory_...  2.18 us

profile of v5, /device:TPU:40, one launch (start us, length us, event | category | flops | bytes accessed | tf_op | source)
XLA Modules:
  0.0 63.2 jit_solution(11351723122647974259)
XLA Ops:
  0.6 60.4 %layer.1 = (bf16[8,1024]{1,0:T(8,128)(2,1)S(1)}, f32[8,16,64,64]{3,2,1,0:T(8,128)S(1)}, bf16[3,8,1024]{2,1,0:T(8,128)(2,1)S(1)}) custom-call(bf16[8,1024]{1,0:T(8,128)(2,1)} %hidden_h.1, bf16[8,1024]{1,0:T(8,128)(2,1)} %head_in_h.1, bf16[8,1024]{1,0:T(8,128)(2,1)} %gate_h.1, bf16[8,128]{1,0:T(8,128)(2,1)} %b_map_h.1, bf16[8,128]{1,0:T(8,128)(2,1)} %c_map_h.1, ...), custom_call_target="tpu_custom_call" | custom-call | tf_op jit(solution)/shard_map/layer/pallas_call | solution.py:374
  61.0 2.2 %store.1 = (bf16[8,1024]{1,0:T(8,128)(2,1)}, f32[8,16,64,64]{3,2,1,0:T(8,128)}, bf16[3,8,1024]{2,1,0:T(8,128)(2,1)}) custom-call(bf16[8,1024]{1,0:T(8,128)(2,1)S(1)} %get-tuple-element.9.refs_0_, f32[8,16,64,64]{3,2,1,0:T(8,128)S(1)} %get-tuple-element.10.refs_1_, bf16[3,8,1024]{2,1,0:T(8,128)(2,1)S(1)} %get-tuple-element.11.refs_2_), custom_call_target="tpu_custom_call" | custom-call | tf_op jit(solution)/shard_map/store/pallas_call | solution.py:423

commit v6 on v5

--- a/solution.py
+++ b/solution.py
@@ -193,15 +193,22 @@
                     h = g * per_group + j
                     new_state[s, h] = decay[s : s + 1, h : h + 1] * state[s, h] + outer[j * width : (j + 1) * width]
 
-    copies, arrived = [], {}
+    direct = [hop % nz for hop in FIRST[0][1] if hop % nz not in [origin for origin, _ in FAN]]
+
+    def first_for(block):
+        for i, (origin, _) in enumerate(FAN):
+            if block == origin:
+                return i
+        return 2 if block in direct else 3
+
+    def token_wait(count, at):
+        some_blocks = tokens.at[pl.ds(0, count)]
+        return remote(some_blocks, some_blocks, z_s, z_r.at[at], partner)
 
     def spread_from(origin, hops):
         for hop in hops:
-            q = len(copies)
             lands = (origin + hop) % nz
-            copies.append(remote(tokens.at[spot(origin)], tokens.at[spot(lands)], z_s.at[q], z_r.at[q], along_z(hop)))
-            arrived[lands] = copies[q]
-            copies[q].start()
+            remote(tokens.at[spot(origin)], tokens.at[spot(lands)], z_s, z_r.at[first_for(lands)], along_z(hop)).start()
 
     for origin, hops in FIRST:
         spread_from(origin, hops)
@@ -211,15 +218,17 @@
     for copy in keep[:2]:
         copy.start()
     for origin, hops in FAN:
-        arrived.pop(origin).wait_recv()
+        token_wait(1, first_for(origin)).wait_recv()
         spread_from(origin, hops)
 
     def at_x(ref, part, d):
         return ref.at[part, (x + d + X_SIDE) % X_SIDE]
 
     def across(part):
-        for block in [b for b in arrived if part or {b, nz - b} & set(BLOCKS[:some])]:
-            arrived.pop(block).wait_recv()
+        if part:
+            token_wait(nz - 1 - len(FAN) - len(direct), 3).wait_recv()
+        else:
+            token_wait(len(direct), 2).wait_recv()
         held = tokens[part * some : (part + 1) * some].astype(F32).reshape(some * seqs, half + LANES)
         info = held[:, half:]
         info = info + jnp.where(iota(info.shape, 1) < TOPK, 0.0, pltpu.roll(info, LANES - TOPK, 1))
@@ -239,10 +248,10 @@
         pick_tx[part] = picked.reshape(X_SIDE, slots, half)
         sent = []
         for i, d in enumerate(ORDER):
-            sent.append(remote(at_x(pick_tx, part, d), pick_rx.at[part, x], x_s.at[part, i], x_r.at[part, i], along_x(d)))
+            sent.append(remote(at_x(pick_tx, part, d), pick_rx.at[part, x], x_s.at[part], x_r.at[part, i], along_x(d)))
             sent[i].start()
         pick_rx[part, x] = pick_tx[part, x]
-        shared = [remote(pick_tx.at[part, x], pick_other.at[part, x], o_s.at[part, 3], o_r.at[part, 3], partner)]
+        shared = [remote(pick_tx.at[part, x], pick_other.at[part, x], o_s.at[part], o_r.at[part], partner)]
         shared[0].start()
         return sent, shared, (mix_hi, mix_lo)
 
@@ -250,8 +259,8 @@
         for i in (1, 2, 0):
             d = ORDER[i]
             got = at_x(pick_rx, part, -d)
-            remote(got, got, x_s.at[part, i], x_r.at[part, i], along_x(d)).wait_recv()
-            shared.append(remote(got, at_x(pick_other, part, -d), o_s.at[part, i], o_r.at[part, i], partner))
+            remote(got, got, x_s.at[part], x_r.at[part, i], along_x(d)).wait_recv()
+            shared.append(remote(got, at_x(pick_other, part, -d), o_s.at[part], o_r.at[part], partner))
             shared[-1].start()
 
     def project(values, cols):
@@ -264,8 +273,7 @@
 
     def activate(part, shared):
         g0, u0, s0 = project(pick_rx[part], mine_cols)
-        for copy in shared:
-            copy.wait_recv()
+        remote(pick_rx.at[part], pick_other.at[part], o_s.at[part], o_r.at[part], partner).wait_recv()
         g1, u1, s1 = project(pick_other[part], other_cols)
         inv = lax.rsqrt((s0 + s1) / (2 * half) + EPSILON)
         return (silu(inv * (g0 + g1)) * (inv * (u0 + u1))).astype(BF16)
@@ -282,15 +290,17 @@
         back_tx[part] = result.reshape(X_SIDE, slots, half)
         returned = []
         for i, d in enumerate(ORDER):
-            returned.append(remote(at_x(back_tx, part, d), back_rx.at[part, x], b_s.at[part, i], b_r.at[part, i], along_x(d)))
+            returned.append(remote(at_x(back_tx, part, d), back_rx.at[part, x], b_s.at[part], b_r.at[part], along_x(d)))
             returned[i].start()
         back_rx[part, x] = back_tx[part, x]
         return returned
 
+    def three_backs(part):
+        blocks = pl.ds(0, X_SIDE - 1)
+        return remote(back_tx.at[part, blocks], back_rx.at[part, blocks], b_s.at[part], b_r.at[part], partner)
+
     def collect(part, mix):
-        for i, d in enumerate(ORDER):
-            got = at_x(back_rx, part, -d)
-            remote(got, got, b_s.at[part, i], b_r.at[part, i], along_x(d)).wait_recv()
+        three_backs(part).wait_recv()
         rows_back = back_rx[part].reshape(rows, half)
         total = jnp.dot(mix[0], rows_back, preferred_element_type=F32) + jnp.dot(mix[1], rows_back, preferred_element_type=F32)
         total = total.reshape(some, seqs, half)
@@ -310,47 +320,45 @@
     returned_f = back(1, trade_f, own_f)
     returned_n = back(0, trade_n, own_n)
 
-    parts = []
-
-    def send(src, dst, hop):
-        q = len(parts)
-        parts.append(remote(src, dst, h_s.at[q], h_r.at[q], along_z(hop)))
-        parts[q].start()
-        return parts[q]
-
-    gathered = {origin: [] for origin, _ in FAN}
-
-    def send_far(part):
-        for origin, hops in FAN:
-            for hop in hops:
-                block = (origin + hop) % nz
-                if PLACE[block] // some == part:
-                    n = sum(len(g) for g in gathered.values())
-                    gathered[origin].append((send(sums_bf.at[spot(block)], relay_rx.at[n], -hop), n))
+    def send(src, dst, hop, at):
+        remote(src, dst, h_s, h_r.at[at], along_z(hop)).start()
+
+    def sum_wait(count, at):
+        some_blocks = sums_bf.at[pl.ds(0, count)]
+        return remote(some_blocks, some_blocks, h_s, h_r.at[at], partner)
+
+    (_, first_hops), = FIRST
+    counts = [len(hops) for _, hops in FAN]
 
     collect(1, mix_f)
-    send_far(1)
+    for i, (origin, hops) in enumerate(FAN):
+        for n, hop in enumerate(hops):
+            send(sums_bf.at[spot((origin + hop) % nz)], relay_rx.at[sum(counts[:i]) + n], -hop, i)
     collect(0, mix_n)
-    send_far(0)
-    finals = []
-    (_, first_hops), = FIRST
-    for i, (origin, _) in enumerate(FAN):
+    for i, (origin, hops) in enumerate(FAN):
+        sum_wait(counts[i], i).wait_recv()
         total = sums[spot(origin)]
-        for copy, at in gathered[origin]:
-            copy.wait_recv()
-            total = total + relay_rx[at].astype(F32)
+        for n in range(counts[i]):
+            total = total + relay_rx[sum(counts[:i]) + n].astype(F32)
         relay_tx[i] = total.astype(BF16)
-        finals.append(send(relay_tx.at[i], last_rx.at[len(finals)], -first_hops[i]))
-    for hop in first_hops[len(FAN):]:
-        finals.append(send(sums_bf.at[spot(hop % nz)], last_rx.at[len(finals)], -hop))
+        send(relay_tx.at[i], last_rx.at[i], -first_hops[i], 2)
+    for i, hop in enumerate(first_hops[len(FAN) :]):
+        send(sums_bf.at[spot(hop % nz)], last_rx.at[len(FAN) + i], -hop, 2)
     total = resid.astype(F32) + sums[0]
-    for i, copy in enumerate(finals):
-        copy.wait_recv()
+    sum_wait(len(first_hops), 2).wait_recv()
+    for i in range(len(first_hops)):
         total = total + last_rx[i].astype(F32)
     out[...] = total.astype(BF16)
     keep[2].start()
-    for copy in [*copies, *sent_n, *sent_f, *shared_n, *shared_f, trade_n, trade_f, *returned_n, *returned_f, *parts]:
-        copy.wait_send()
+    token_wait(nz - 1, 0).wait_send()
+    sum_wait(nz - 1, 0).wait_send()
+    for part in range(2):
+        three = pick_tx.at[part, pl.ds(0, X_SIDE - 1)]
+        remote(three, three, x_s.at[part], x_r.at[part, 0], partner).wait_send()
+        remote(pick_rx.at[part], pick_other.at[part], o_s.at[part], o_r.at[part], partner).wait_send()
+        three_backs(part).wait_send()
+    trade_n.wait_send()
+    trade_f.wait_send()
     for copy in keep:
         copy.wait()
 
@@ -398,8 +406,8 @@
             pltpu.VMEM((far, seqs, half), BF16),
             pltpu.VMEM((2, seqs, half), BF16),
             pltpu.VMEM((near, seqs, half), BF16),
-            dma((14 + seqs,)), dma((7,)), one, one, dma((nz - 1,)), dma((nz - 1,)), dma((2, 3)), dma((2, 3)), dma((2, 4)), dma((2, 4)),
-            dma((2,)), dma((2,)), dma((2, 3)), dma((2, 3)), dma((nz - 1,)), dma((nz - 1,)),
+            dma((14 + 4,)), dma((7,)), one, one, one, dma((4,)), dma((2,)), dma((2, 3)), dma((2,)), dma((2,)),
+            dma((2,)), dma((2,)), dma((2,)), dma((2,)), one, dma((3,)),
         ],
         compiler_params=pltpu.CompilerParams(collective_id=0, has_side_effects=True, vmem_limit_bytes=VMEM_BYTES),
     )(*(pltpu.with_memory_space_constraint(a, pltpu.HBM) for a in args))
@@ -407,16 +415,14 @@
 
 def store_kernel(*refs):
     count = (len(refs) - 1) // 2
-    sem = refs[-1]
-    copies = []
-    for src, dst in zip(refs[:count], refs[count:-1]):
+    pairs = list(zip(refs[:count], refs[count:-1]))
+    for at, (src, dst) in enumerate(pairs):
         pieces = src.shape[0] if src.ndim == 4 else 1
         for i in range(pieces):
             piece = pl.ds(i * (src.shape[0] // pieces), src.shape[0] // pieces)
-            copies.append(pltpu.make_async_copy(src.at[piece], dst.at[piece], sem.at[len(copies)]))
-            copies[-1].start()
-    for copy in copies:
-        copy.wait()
+            pltpu.make_async_copy(src.at[piece], dst.at[piece], refs[-1].at[at]).start()
+    for at, (src, dst) in enumerate(pairs):
+        pltpu.make_async_copy(src, dst, refs[-1].at[at]).wait()
 
 
 def store(*values):
@@ -426,7 +432,7 @@
         in_specs=[pl.BlockSpec(memory_space=pl.ANY)] * len(values),
         out_specs=[pl.BlockSpec(memory_space=pltpu.HBM)] * len(values),
         out_shape=[pltpu.HBM(v.shape, v.dtype) for v in values],
-        scratch_shapes=[pltpu.SemaphoreType.DMA((sum(v.shape[0] for v in values),))],
+        scratch_shapes=[pltpu.SemaphoreType.DMA((len(values),))],
         compiler_params=pltpu.CompilerParams(vmem_limit_bytes=VMEM_BYTES),
     )(*(pltpu.with_memory_space_constraint(v, pltpu.VMEM) for v in values))
 

time: 63.3 us -> 62.3 us (0.984)
  Pallas kernels: 62.6 us -> 61.6 us
    pallas_call x1, Pallas kernels: 60.4 us -> 59.6 us  [layer(): pl.pallas_call(layer_kernel, name='layer', in_specs=[hbm] * len(args), ou...]
where the time goes in v6:
time: 62.3 us; the launch traced here: 62.2 us
  Pallas kernels  61.6 us (99%)
  between operations  0.65 us (1%)
    pallas_call x1, Pallas kernels, layer(): pl.pallas_call(layer_kernel, name='layer', in_specs=[hbm] * len(args), ou...  59.6 us
    pallas_call x1, Pallas kernels, store(): pl.pallas_call(store_kernel, name='store', in_specs=[pl.BlockSpec(memory_...  2.03 us

profile of v6, /device:TPU:40, one launch (start us, length us, event | category | flops | bytes accessed | tf_op | source)
XLA Modules:
  0.0 62.2 jit_solution(9711888421984803123)
XLA Ops:
  0.6 59.6 %layer.1 = (bf16[8,1024]{1,0:T(8,128)(2,1)S(1)}, f32[8,16,64,64]{3,2,1,0:T(8,128)S(1)}, bf16[3,8,1024]{2,1,0:T(8,128)(2,1)S(1)}) custom-call(bf16[8,1024]{1,0:T(8,128)(2,1)} %hidden_h.1, bf16[8,1024]{1,0:T(8,128)(2,1)} %head_in_h.1, bf16[8,1024]{1,0:T(8,128)(2,1)} %gate_h.1, bf16[8,128]{1,0:T(8,128)(2,1)} %b_map_h.1, bf16[8,128]{1,0:T(8,128)(2,1)} %c_map_h.1, ...), custom_call_target="tpu_custom_call" | custom-call | tf_op jit(solution)/shard_map/layer/pallas_call | solution.py:382
  60.2 2.0 %store.1 = (bf16[8,1024]{1,0:T(8,128)(2,1)}, f32[8,16,64,64]{3,2,1,0:T(8,128)}, bf16[3,8,1024]{2,1,0:T(8,128)(2,1)}) custom-call(bf16[8,1024]{1,0:T(8,128)(2,1)S(1)} %get-tuple-element.9.refs_0_, f32[8,16,64,64]{3,2,1,0:T(8,128)S(1)} %get-tuple-element.10.refs_1_, bf16[3,8,1024]{2,1,0:T(8,128)(2,1)S(1)} %get-tuple-element.11.refs_2_), custom_call_target="tpu_custom_call" | custom-call | tf_op jit(solution)/shard_map/store/pallas_call | solution.py:429

commit v7 on v6

--- a/solution.py
+++ b/solution.py
@@ -147,13 +147,6 @@
             src_ref=src, dst_ref=dst, send_sem=send, recv_sem=recv, device_id=peer, device_id_type=MESH
         )
 
-    get_wout.wait()
-    tp_tx[...] = jnp.dot(gated, wout[:, other_cols], preferred_element_type=F32).astype(BF16)
-    pl.semaphore_wait(barrier, len(peers))
-    swap = remote(tp_tx, tp_rx, tp_s, tp_r, partner)
-    swap.start()
-    own_mix = jnp.dot(gated, wout[:, mine_cols], preferred_element_type=F32).astype(BF16)
-
     idx = chosen[...]
     wts = weights[...]
     lane = iota((seqs, LANES), 1)
@@ -173,6 +166,13 @@
         extra = jnp.where(lane == TOPK + i, w_hi, extra)
         extra = jnp.where(lane == 2 * TOPK + i, w - w_hi, extra)
     tokens[0, :, half:] = extra.astype(BF16)
+
+    get_wout.wait()
+    tp_tx[...] = jnp.dot(gated, wout[:, other_cols], preferred_element_type=F32).astype(BF16)
+    pl.semaphore_wait(barrier, len(peers))
+    swap = remote(tp_tx, tp_rx, tp_s, tp_r, partner)
+    swap.start()
+    own_mix = jnp.dot(gated, wout[:, mine_cols], preferred_element_type=F32).astype(BF16)
 
     base = hidden[...].astype(F32)
     swap.wait()

time: 62.3 us -> 62.3 us (level)
  no operation moved by 1% of the time
where the time goes in v7:
time: 62.3 us; the launch traced here: 62.2 us
  Pallas kernels  61.6 us (99%)
  between operations  0.65 us (1%)
    pallas_call x1, Pallas kernels, layer(): pl.pallas_call(layer_kernel, name='layer', in_specs=[hbm] * len(args), ou...  59.6 us
    pallas_call x1, Pallas kernels, store(): pl.pallas_call(store_kernel, name='store', in_specs=[pl.BlockSpec(memory_...  2.03 us

profile of v7, /device:TPU:40, one launch (start us, length us, event | category | flops | bytes accessed | tf_op | source)
XLA Modules:
  0.0 62.2 jit_solution(3629044439787996839)
XLA Ops:
  0.6 59.6 %layer.1 = (bf16[8,1024]{1,0:T(8,128)(2,1)S(1)}, f32[8,16,64,64]{3,2,1,0:T(8,128)S(1)}, bf16[3,8,1024]{2,1,0:T(8,128)(2,1)S(1)}) custom-call(bf16[8,1024]{1,0:T(8,128)(2,1)} %hidden_h.1, bf16[8,1024]{1,0:T(8,128)(2,1)} %head_in_h.1, bf16[8,1024]{1,0:T(8,128)(2,1)} %gate_h.1, bf16[8,128]{1,0:T(8,128)(2,1)} %b_map_h.1, bf16[8,128]{1,0:T(8,128)(2,1)} %c_map_h.1, ...), custom_call_target="tpu_custom_call" | custom-call | tf_op jit(solution)/shard_map/layer/pallas_call | solution.py:382
  60.2 2.0 %store.1 = (bf16[8,1024]{1,0:T(8,128)(2,1)}, f32[8,16,64,64]{3,2,1,0:T(8,128)}, bf16[3,8,1024]{2,1,0:T(8,128)(2,1)}) custom-call(bf16[8,1024]{1,0:T(8,128)(2,1)S(1)} %get-tuple-element.9.refs_0_, f32[8,16,64,64]{3,2,1,0:T(8,128)S(1)} %get-tuple-element.10.refs_1_, bf16[3,8,1024]{2,1,0:T(8,128)(2,1)S(1)} %get-tuple-element.11.refs_2_), custom_call_target="tpu_custom_call" | custom-call | tf_op jit(solution)/shard_map/store/pallas_call | solution.py:429
